TPU v7x, 512 devices: a whole 4x4x16 slice. The times are simulated.
512 devices in a mesh: sp: 64 (over z, y), tp: 8 (over x, core).
Axes of the slice: x: 4, y: 4, z: 16, core: 2. Of those that a mesh axis runs over, the one named last changes fastest.
Arguments:
- tokens: bfloat16 [16384, 2048], P('sp'), may hold values from -6 to 6
- ln_gain: float32 [2048], replicated, may hold values from 0.1 to 1.9
- w_query_attn: bfloat16 [2048, 1024], P('sp', 'tp'), may hold values from -0.125 to 0.125
- w_key_attn: bfloat16 [2048, 1024], P('sp', 'tp'), may hold values from -0.125 to 0.125
- w_value_attn: bfloat16 [2048, 1024], P('sp', 'tp'), may hold values from -0.125 to 0.125
- w_query_delta: bfloat16 [2048, 1024], P('sp', 'tp'), may hold values from -0.125 to 0.125
- w_key_delta: bfloat16 [2048, 1024], P('sp', 'tp'), may hold values from -0.125 to 0.125
- w_value_delta: bfloat16 [2048, 1024], P('sp', 'tp'), may hold values from -0.125 to 0.125
- w_beta: bfloat16 [2048, 8], replicated, may hold values from -0.125 to 0.125
- w_decay: bfloat16 [2048, 8], replicated, may hold values from -0.125 to 0.125
- attn_bias: float32 [16], replicated, may hold values from -13 to 1
- decay_log: float32 [8], replicated, may hold values from -15 to -2
- beta_bias: float32 [8], replicated, may hold values from -7 to 1
- log_decay_extra: float32 [16384, 8], P('sp', 'tp'), may hold values from -0.7 to 0, as said below
- attn_gain: float32 [64], replicated, may hold values from 0.1 to 1.9
- delta_gain: float32 [128], replicated, may hold values from 0.1 to 1.9
- w_out_attn: bfloat16 [1024, 2048], P('tp', 'sp'), may hold values from -0.125 to 0.125
- w_out_delta: bfloat16 [1024, 2048], P('tp', 'sp'), may hold values from -0.125 to 0.125
Outputs:
- mixed_out: bfloat16 [16384, 2048], P(('sp', 'tp'))
Inputs may be any that keep to these rules, and one draw needn't show every extreme that they name: `log_decay_extra`: never positive.
All inputs are finite; a program needn't handle non-finite values.
Results may differ from a plain program's by a relative error of at most 0.015.
Values may be sent and summed in bfloat16 or wider, within the bound.
A program may use at most 128 MiB of HBM per device.

v0:
```python
import math

import jax
import jax.numpy as jnp
from jax import lax
from jax.sharding import Mesh
from jax.sharding import PartitionSpec as P

SB_DIM = 64
GDN_DIM = 128
DBLOCK = 64
SP = ("sp_0", "sp_1")
SP_TP = ("sp_0", "sp_1", "tp")


def side_by_side(arrays, axis, dim, along):
    widths = [a.shape[along] for a in arrays]
    both = jnp.concatenate(arrays, axis=along)
    result = lax.all_gather(both, axis, axis=dim, tiled=True)
    return tuple(jnp.split(result, [sum(widths[:k]) for k in range(1, len(widths))], axis=along))


def neutral_like(value, identity):
    return jax.tree.map(
        lambda a, e: jnp.broadcast_to(jnp.asarray(e, a.dtype), a.shape), value, identity
    )


def carried_in(value, axes, combine, identity):
    before = start = neutral_like(value, identity)
    running = value
    for axis in reversed(axes):
        length, index = (lax.axis_size(axis), lax.axis_index(axis))
        pieces = jax.tree.map(lambda part: lax.all_gather(part, axis), running)
        inside, running = (start, start)
        for k in range(length):
            passed = k < index
            running = combine(running, jax.tree.map(lambda part: part[k], pieces))
            inside = jax.tree.map(lambda new, old: jnp.where(passed, new, old), running, inside)
        before = combine(inside, before)
    return before


def turned_gather(arrays, axis, dims):
    turned = [jnp.moveaxis(a, dim, 0) for a, dim in zip(arrays, dims)]
    widths = [t[0].size for t in turned]
    both = jnp.concatenate([t.reshape(-1, w) for t, w in zip(turned, widths)], axis=1)
    result = lax.all_gather(both, axis, axis=0, tiled=True)
    pieces = jnp.split(result, [sum(widths[:k]) for k in range(1, len(widths))], axis=1)
    return tuple(
        (
            jnp.moveaxis(b.reshape(-1, *t.shape[1:]), 0, dim)
            for b, t, dim in zip(pieces, turned, dims)
        )
    )


def cut_along(value, dim, length):
    before, after = (value.shape[:dim], value.shape[dim + 1 :])
    return jnp.moveaxis(value.reshape(*before, length, -1, *after), dim, 0)


def summed_on_arrival(value, axis, dim):
    length = lax.axis_size(axis)
    pieces = lax.all_to_all(cut_along(value, dim, length), axis, 0, 0, tiled=True)
    return jnp.sum(pieces.astype(jnp.float32), axis=0)


def layer_normed(tok_rows, ln_gain):
    values = tok_rows.astype(jnp.float32)
    center = jnp.mean(values, axis=-1, keepdims=True)
    spread = jnp.mean(jnp.square(values - center), axis=-1, keepdims=True)
    return ((values - center) * lax.rsqrt(spread + 1e-05) * ln_gain).astype(jnp.bfloat16)


def rms_scaled(values, gain):
    return values * lax.rsqrt(jnp.mean(jnp.square(values), axis=-1, keepdims=True) + 1e-06) * gain


def unit_rows(values):
    return values * lax.rsqrt(jnp.sum(jnp.square(values), axis=-1, keepdims=True) + 1e-06)


def stick_block(carry, queries, query_pos, head_bias, key_block, value_block, key_first):
    outputs, log_kept = carry
    key_count = key_block.shape[0]
    heads = queries.shape[1]
    head_width = queries.shape[2]
    scores = jnp.einsum(
        "rhd,khd->hrk",
        queries,
        key_block.reshape(key_count, heads, head_width),
        preferred_element_type=jnp.float32,
    )
    scores = scores * head_width ** (-0.5) + head_bias[:, None, None]
    key_pos = key_first + jnp.arange(key_count, dtype=jnp.int32)
    visible = (key_pos[None, :] < query_pos[:, None]) & (key_pos[None, :] >= 0)
    lost = jnp.where(visible[None], -jax.nn.softplus(scores), 0.0)
    between = lax.cumsum(lost, axis=2, reverse=True) - lost + log_kept[:, :, None]
    weights = jnp.where(visible[None], jnp.exp(jax.nn.log_sigmoid(scores) + between), 0.0).astype(
        jnp.bfloat16
    )
    outputs = outputs + jnp.einsum(
        "hrk,khd->hrd",
        weights,
        value_block.reshape(key_count, heads, head_width),
        preferred_element_type=jnp.float32,
    )
    return (outputs, log_kept + jnp.sum(lost, axis=2))


def stick_span(carry, queries, query_pos, head_bias, keys, values, key_first):
    own_rows = queries.shape[0]
    length = keys.shape[0]
    widest = max(1, 1024 // own_rows)
    widest = 1 << widest.bit_length() - 1
    block = own_rows * math.gcd(widest, length // own_rows)
    blocks = length // block

    def one_turn(step_index, inner):
        block_index = blocks - 1 - step_index
        key_block = lax.dynamic_slice_in_dim(keys, block_index * block, block, 0)
        value_block = lax.dynamic_slice_in_dim(values, block_index * block, block, 0)
        return stick_block(
            inner,
            queries,
            query_pos,
            head_bias,
            key_block,
            value_block,
            key_first + block_index * block,
        )

    return lax.fori_loop(0, blocks, one_turn, carry)


def delta_parts(queries, keys, values, beta, decay):
    width = queries.shape[-2]
    key_width = queries.shape[-1]
    decay_sum = jnp.cumsum(decay, axis=-1)
    lower = jnp.tril(jnp.ones((width, width), dtype=bool))
    strict = jnp.tril(jnp.ones((width, width), dtype=bool), -1)
    differ = decay_sum[..., :, None] - decay_sum[..., None, :]
    decay_mask = jnp.where(lower, jnp.exp(jnp.where(lower, differ, 0.0)), 0.0)
    keys_beta = keys * beta[..., None]
    values_beta = values * beta[..., None]
    strict_mat = jnp.where(
        strict, jnp.einsum("...id,...jd->...ij", keys_beta, keys) * decay_mask, 0.0
    )
    right_side = jnp.concatenate([keys_beta * jnp.exp(decay_sum)[..., None], values_beta], axis=-1)
    solved = jax.scipy.linalg.solve_triangular(
        jnp.eye(width, dtype=jnp.float32) + strict_mat, right_side, lower=True
    )
    solve_keys = solved[..., :key_width]
    solve_values = solved[..., key_width:]
    query_key = jnp.einsum("...id,...jd->...ij", queries, keys) * decay_mask
    query_decayed = queries * jnp.exp(decay_sum)[..., None]
    keys_to_end = keys * jnp.exp(decay_sum[..., -1:] - decay_sum)[..., None]
    block_decay = jnp.exp(decay_sum[..., -1])
    return (solve_keys, solve_values, query_decayed, query_key, keys_to_end, block_decay)


def delta_update(state, block_parts):
    solve_keys, solve_values, query_decayed, query_key, keys_to_end, block_decay = block_parts
    fresh = solve_values - jnp.einsum("hcd,hde->hce", solve_keys, state)
    outputs = jnp.einsum("hcd,hde->hce", query_decayed, state)
    outputs = outputs + jnp.einsum("hij,hje->hie", query_key, fresh)
    state = state * block_decay[:, None, None] + jnp.einsum("hcd,hce->hde", keys_to_end, fresh)
    return (state, outputs)


def chain_combine(earlier, later):
    earlier_map, earlier_state = earlier
    later_map, later_state = later
    joined_map = jnp.einsum("hij,hjk->hik", later_map, earlier_map)
    joined_state = jnp.einsum("hij,hjk->hik", later_map, earlier_state) + later_state
    return (joined_map, joined_state)


def local(
    tokens,
    ln_gain,
    w_query_attn,
    w_key_attn,
    w_value_attn,
    w_query_delta,
    w_key_delta,
    w_value_delta,
    w_beta,
    w_decay,
    attn_bias,
    decay_log,
    beta_bias,
    log_decay_extra,
    attn_gain,
    delta_gain,
    w_out_attn,
    w_out_delta,
):
    row_count = tokens.shape[0]
    normed = layer_normed(tokens, ln_gain)
    segments = side_by_side(
        (w_query_attn, w_key_attn, w_value_attn, w_query_delta, w_key_delta, w_value_delta),
        SP,
        0,
        1,
    )
    summed = tuple(
        (jnp.dot(normed, segment, preferred_element_type=jnp.float32) for segment in segments)
    )
    attn_query, attn_key, attn_value, delta_query, delta_key, delta_value = [
        result.astype(jnp.bfloat16) for result in summed
    ]
    tp_pos = lax.axis_index("tp")
    sp_pos = lax.axis_index(SP)
    attn_heads = attn_query.shape[1] // SB_DIM
    delta_heads = delta_query.shape[1] // GDN_DIM
    positions = sp_pos * row_count + jnp.arange(row_count, dtype=jnp.int32)
    queries = attn_query.reshape(row_count, attn_heads, SB_DIM)
    head_bias = lax.dynamic_slice_in_dim(attn_bias, tp_pos * attn_heads, attn_heads, 0)
    carry = (
        jnp.zeros((attn_heads, row_count, SB_DIM), jnp.float32),
        jnp.zeros((attn_heads, row_count), jnp.float32),
    )
    every_key, every_value = side_by_side((attn_key, attn_value), SP, 0, 1)
    carry = stick_span(carry, queries, positions, head_bias, every_key, every_value, 0)
    attn_mixed = rms_scaled(carry[0], attn_gain).astype(jnp.bfloat16)
    head_first = tp_pos * delta_heads
    beta_cols = lax.dynamic_slice_in_dim(w_beta, head_first, delta_heads, 1)
    decay_cols = lax.dynamic_slice_in_dim(w_decay, head_first, delta_heads, 1)
    beta_pre = jnp.dot(normed, beta_cols, preferred_element_type=jnp.float32).astype(jnp.bfloat16)
    decay_pre = jnp.dot(normed, decay_cols, preferred_element_type=jnp.float32).astype(jnp.bfloat16)
    queries = unit_rows(
        jax.nn.silu(delta_query.astype(jnp.float32)).reshape(row_count, delta_heads, GDN_DIM)
    ) * GDN_DIM ** (-0.5)
    keys = unit_rows(
        jax.nn.silu(delta_key.astype(jnp.float32)).reshape(row_count, delta_heads, GDN_DIM)
    )
    values = jax.nn.silu(delta_value.astype(jnp.float32)).reshape(row_count, delta_heads, GDN_DIM)
    beta = jax.nn.sigmoid(
        beta_pre.astype(jnp.float32)
        + lax.dynamic_slice_in_dim(beta_bias, head_first, delta_heads, 0)
    )
    rates = jnp.exp(lax.dynamic_slice_in_dim(decay_log, head_first, delta_heads, 0))
    decay = -rates * jax.nn.softplus(decay_pre.astype(jnp.float32)) + log_decay_extra
    blocks = row_count // DBLOCK

    def to_blocks(array):
        return jnp.moveaxis(array.reshape((blocks, DBLOCK) + array.shape[1:]), 2, 0)

    parts = delta_parts(
        to_blocks(queries), to_blocks(keys), to_blocks(values), to_blocks(beta), to_blocks(decay)
    )
    sequence = tuple((jnp.moveaxis(piece_part, 1, 0) for piece_part in parts))
    eye_mat = jnp.eye(GDN_DIM, dtype=jnp.float32)

    def carry_map(accum, block_parts):
        transition, written = accum
        solve_keys, solve_values, query_decayed, query_key, keys_to_end, block_decay = block_parts
        step_matrix = block_decay[:, None, None] * eye_mat - jnp.einsum(
            "hcd,hce->hde", keys_to_end, solve_keys
        )
        transition = jnp.einsum("hij,hjk->hik", step_matrix, transition)
        written = jnp.einsum("hij,hjk->hik", step_matrix, written)
        written = written + jnp.einsum("hcd,hce->hde", keys_to_end, solve_values)
        return ((transition, written), None)

    neutral = (
        jnp.broadcast_to(eye_mat, (delta_heads, GDN_DIM, GDN_DIM)),
        jnp.zeros((delta_heads, GDN_DIM, GDN_DIM), jnp.float32),
    )
    own_chain, _ = lax.scan(carry_map, neutral, sequence)
    _, incoming = carried_in(own_chain, SP, chain_combine, neutral)
    _, outputs = lax.scan(delta_update, incoming, sequence)
    delta_raw = jnp.moveaxis(outputs, 0, 1).reshape(delta_heads, row_count, GDN_DIM)
    delta_mixed = rms_scaled(delta_raw, delta_gain).astype(jnp.bfloat16)
    full_attn, full_delta = turned_gather((w_out_attn, w_out_delta), SP, (1, 1))
    attn_weight3 = full_attn.reshape(attn_heads, SB_DIM, full_attn.shape[1])
    delta_weight3 = full_delta.reshape(delta_heads, GDN_DIM, full_delta.shape[1])
    result = jnp.einsum("hrd,hdn->rn", attn_mixed, attn_weight3, preferred_element_type=jnp.float32)
    mixed_rows = summed_on_arrival(
        (
            result
            + jnp.einsum(
                "hrd,hdn->rn", delta_mixed, delta_weight3, preferred_element_type=jnp.float32
            )
        ).astype(jnp.bfloat16),
        "tp",
        0,
    )
    return mixed_rows.astype(jnp.bfloat16)


def solution(mesh):
    split = Mesh(mesh.devices.reshape(16, 4, mesh.shape["tp"]), ("sp_0", "sp_1", "tp"))
    return jax.shard_map(
        local,
        mesh=split,
        in_specs=(
            P(SP, None),
            P(),
            P(SP, "tp"),
            P(SP, "tp"),
            P(SP, "tp"),
            P(SP, "tp"),
            P(SP, "tp"),
            P(SP, "tp"),
            P(),
            P(),
            P(),
            P(),
            P(),
            P(SP, "tp"),
            P(),
            P(),
            P("tp", SP),
            P("tp", SP),
        ),
        out_specs=P(SP_TP, None),
        check_vma=False,
    )
```

profile of v0, /device:TPU:1, one launch (start us, length us, event | category | flops | bytes accessed | tf_op | source)
XLA Modules:
  0.0 829.6 jit_solution(2809152960668360981)
XLA Ops:
  21.7 129.8 %all-gather.9.cloned.1.call-done = bf16[2048,768]{1,0:T(8,128)(2,1)} async-done(((bf16[32,768]{1,0:T(8,128)(2,1)}), bf16[2048,768]{1,0:T(8,128)(2,1)}) %all-gather.9.cloned.1.call-update) | async-done | bytes 3145744 | tf_op jit(solution)/shard_map/all_gather | solution.py:19
  153.3 19.7 %custom-call.4 = f32[4,1,64,64]{2,3,1,0:T(8,128)S(1)} custom-call(f32[4,1,64,64]{3,2,1,0:T(8,128)S(1)} %fusion.60), custom_call_target="InvertDiagBlocksLowerTriangular" | custom-call | tf_op jit(solution)/shard_map/jit(_solve_triangular)/vmap()/triangular_solve | solution.py:151
  175.2 7.6 while.42
  182.9 9.2 %all-gather = bf16[4,128,128]{2,1,0:T(8,128)(2,1)S(1)} all-gather(bf16[1,128,128]{2,1,0:T(8,128)(2,1)S(1)} %get-tuple-element.235), channel_id=2, replica_groups=mesh['sp_0'=16,'sp_1'=4,'tp'=8] {'sp_1'}, dimensions={0}, use_global_device_ids=true | all-gather | bytes 163840 | tf_op jit(solution)/shard_map/all_gather | solution.py:34
  192.0 9.8 %all-gather.2 = f32[4,128,128]{2,1,0:T(8,128)S(1)} all-gather(f32[1,128,128]{2,1,0:T(8,128)S(1)} %get-tuple-element.236), channel_id=4, replica_groups=mesh['sp_0'=16,'sp_1'=4,'tp'=8] {'sp_1'}, dimensions={0}, use_global_device_ids=true | all-gather | bytes 327680 | tf_op jit(solution)/shard_map/all_gather | solution.py:34
  207.0 81.6 %all-gather.13.cloned.1.call-done = bf16[2048,256]{1,0:T(8,128)(2,1)} async-done(((bf16[32,256]{1,0:T(8,128)(2,1)}), bf16[2048,256]{1,0:T(8,128)(2,1)}) %all-gather.13.cloned.1.call-update) | async-done | bytes 1048592 | tf_op jit(solution)/shard_map/all_gather | solution.py:48
  292.4 23.6 %all-gather.1 = bf16[2048,128]{1,0:T(8,128)(2,1)S(1)} all-gather(bf16[128,128]{1,0:T(8,128)(2,1)S(1)} %fusion.140), channel_id=3, replica_groups=mesh['sp_0'=16,'sp_1'=4,'tp'=8] {'sp_0'}, dimensions={0}, use_global_device_ids=true | all-gather | bytes 557056 | tf_op jit(solution)/shard_map/all_gather | solution.py:34
  317.6 39.7 %all-gather.15.cloned.1.call-done = f32[2048,128]{1,0:T(8,128)} async-done(((f32[128,128]{1,0:T(8,128)}), f32[2048,128]{1,0:T(8,128)}) %all-gather.15.cloned.1.call-update) | async-done | bytes 1048592 | tf_op jit(solution)/shard_map/all_gather | solution.py:34
  373.3 6.9 while.41
  380.5 145.7 %all-gather.11.cloned.1.call-done = bf16[16384,256]{0,1:T(8,128)(2,1)} async-done(((bf16[256,256]{0,1:T(8,128)(2,1)}), bf16[16384,256]{0,1:T(8,128)(2,1)}) %all-gather.11.cloned.1.call-update) | async-done | bytes 8388624 | tf_op jit(solution)/shard_map/all_gather | solution.py:19
  526.2 5.8 fusion.199
  532.0 259.6 %while.43 = (s32[]{:T(128)}, f32[2,256,64]{1,2,0:T(8,128)S(1)}, f32[2,256]{1,0:T(2,128)S(1)}, bf16[16384,128]{0,1:T(8,128)(2,1)}, bf16[256,2,64]{0,2,1:T(8,128)(...) while((s32[]{:T(128)}, f32[2,256,64]{1,2,0:T(8,128)S(1)}, ...), condition=%wide.region_6.7_spmd.clone, body=%wide.region_2.6_spmd.clone.sunk | while | flops 215584000 | bytes 44771616 | solution.py:134
  536.5 5.0 fusion.312
  552.7 5.0 fusion.312
  560.0 4.2 fusion.314
  569.0 5.0 fusion.312
  585.2 5.0 fusion.312
  601.4 5.0 fusion.312
  617.7 5.0 fusion.312
  633.9 5.0 fusion.312
  641.1 4.2 fusion.314
  650.1 5.0 fusion.312
  666.3 5.0 fusion.312
  682.6 5.0 fusion.312
  698.8 5.0 fusion.312
  706.0 4.2 fusion.314
  715.0 5.0 fusion.312
  731.2 5.0 fusion.312
  747.5 5.0 fusion.312
  763.7 5.0 fusion.312
  779.9 5.0 fusion.312
  793.3 28.9 %all_to_all.5 = bf16[8,32,2048]{2,1,0:T(8,128)(2,1)S(1)} all-to-all(bf16[8,32,2048]{2,1,0:T(8,128)(2,1)S(1)} %bitcast.318), channel_id=1, replica_groups=mesh['sp_0'=16,'sp_1'=4,'tp'=8] {'tp'}, dimensions={0} | all-to-all | bytes 2097152 | tf_op jit(solution)/shard_map/all_to_all | solution.py:65
  (449 shorter events, 226.4 us)
Async XLA Ops:
  6.5 11.4 %copy-start = (bf16[2048,8]{0,1:T(8,128)(2,1)S(1)}, bf16[2048,8]{0,1:T(8,128)(2,1)}, u32[]{:S(2)}) copy-start(bf16[2048,8]{0,1:T(8,128)(2,1)} %param.33) | copy-start | bytes 98308
  6.5 11.0 %copy-start.3 = (bf16[256,2048]{1,0:T(8,128)(2,1)S(1)}, bf16[256,2048]{1,0:T(8,128)(2,1)}, u32[]{:S(2)}) copy-start(bf16[256,2048]{1,0:T(8,128)(2,1)} %param.24) | copy-start | bytes 3145732
  6.5 9.6 %copy-start.11 = (f32[8]{0:T(128)S(1)}, f32[8]{0:T(128)}, u32[]{:S(2)}) copy-start(f32[8]{0:T(128)} %param.35) | copy-start | bytes 100
  6.5 11.0 %copy-start.7 = (f32[2048]{0:T(1024)S(1)}, f32[2048]{0:T(1024)}, u32[]{:S(2)}) copy-start(f32[2048]{0:T(1024)} %param.25) | copy-start | bytes 24580
  6.5 144.9 %all-gather.9.cloned.1.call-start = ((), (), s32[]{:S(2)}) async-start(), calls=%async_computation.1 | async-start | bytes 3194880 | tf_op jit(solution)/shard_map/all_gather | solution.py:19
  11.5 277.0 %all-gather.13.cloned.1.call-start = ((), (), s32[]{:S(2)}) async-start(), calls=%async_computation.3 | async-start | bytes 1064960 | tf_op jit(solution)/shard_map/all_gather | solution.py:48
  12.9 344.4 %all-gather.15.cloned.1.call-start = ((), (), s32[]{:S(2)}) async-start(), calls=%async_computation.4 | async-start | bytes 1114112 | tf_op jit(solution)/shard_map/all_gather | solution.py:34
  14.5 3.9 copy-start.8
  17.6 2.6 copy-start.12
  202.0 4.9 copy-start.13
  203.0 323.2 %all-gather.11.cloned.1.call-start = ((), (), s32[]{:S(2)}) async-start(), calls=%async_computation.2 | async-start | bytes 8519680 | tf_op jit(solution)/shard_map/all_gather | solution.py:19
  317.6 55.6 %copy-start.5 = (f32[128,128]{1,0:T(8,128)S(1)}, f32[128,128]{1,0:T(8,128)}, u32[]{:S(2)}) copy-start(f32[128,128]{1,0:T(8,128)} %convolution_add_fusion.20) | copy-start | bytes 196612
  372.0 8.4 %copy-start.9 = (f32[128]{0:T(128)S(1)}, f32[128]{0:T(128)}, u32[]{:S(2)}) copy-start(f32[128]{0:T(128)} %param.39) | copy-start | bytes 1540
  532.0 259.7 %copy-start.10 = (f32[64]{0:T(128)S(1)}, f32[64]{0:T(128)}, u32[]{:S(2)}) copy-start(f32[64]{0:T(128)} %param.38) | copy-start | bytes 772
  536.5 5.0 copy-start.1
  541.8 1.9 copy-start.2
  552.7 5.0 copy-start.1
  558.0 1.9 copy-start.2
  569.0 5.0 copy-start.1
  585.2 5.0 copy-start.1
  601.4 5.0 copy-start.1
  617.7 5.0 copy-start.1
  633.9 5.0 copy-start.1
  650.1 5.0 copy-start.1
  666.3 5.0 copy-start.1
  682.6 5.0 copy-start.1
  698.8 5.0 copy-start.1
  715.0 5.0 copy-start.1
  731.2 5.0 copy-start.1
  747.5 5.0 copy-start.1
  763.7 5.0 copy-start.1
  779.9 5.0 copy-start.1
  (16 other events, 29.0 us)
Sparse Core Ops, SparseCore 0:
  11.7 139.7 all-gather.8
  154.3 134.1 all-gather.12
  290.6 66.6 all-gather.14
  360.1 166.0 all-gather.10
where the time goes:
time: 832 us; the launch traced here: 830 us
  waiting for transfers between devices  397 us (48%)
  other arithmetic  184 us (22%)
  matrix products  93.2 us (11%)
  blocking collectives  71.5 us (9%)
  local copies, waits for them, and re-layouts  67.3 us (8%)
  between operations  14.3 us (2%)
    all_gather x2, waiting for transfers between devices, side_by_side(): result = lax.all_gather(both, axis, axis=dim, tiled=True)  275 us
    all_gather x1, waiting for transfers between devices, turned_gather(): result = lax.all_gather(both, axis, axis=0, tiled=True)  81.6 us
    another operation x32, other arithmetic  81.2 us
    convert_element_type x16, other arithmetic, stick_block(): jnp.where(visible[None], jnp.exp(jax.nn.log_sigmoid(scores) + between), 0.0)  67.1 us
    dot_general x16, matrix products, stick_block(): jnp.einsum('rhd,khd->hrk', queries, key_block.reshape(key_count, heads, h...  48.4 us
    all_gather x3, blocking collectives, carried_in(): pieces = jax.tree.map(lambda part: lax.all_gather(part, axis), running)  42.6 us
    all_gather x1, waiting for transfers between devices, carried_in(): pieces = jax.tree.map(lambda part: lax.all_gather(part, axis), running)  39.7 us
    another operation x16, local copies, waits for them, and re-layouts, stick_block(): lax.cumsum(lost, axis=2, reverse=True) - lost + log_kept[:, :, None]  30.7 us
  transfers between devices with their start and end apart: 4, of which 4 were waited for; matrix products, arithmetic and copies ran while one was open for 9% of the time, Pallas kernels for 0%

commit v1 on v0

v1 whole, which is shorter than its diff:
```python
import functools

import jax
import jax.numpy as jnp
from jax import lax
from jax.experimental import pallas as pl
from jax.experimental.pallas import tpu as pltpu
from jax.sharding import Mesh
from jax.sharding import PartitionSpec as P

MESH = pl.DeviceIdType.MESH
VMEM = pltpu.VMEM
SP = ("z", "y")
LOG2E = 1.4426950408889634
ROWS = 256
F32 = jnp.float32
BF16 = jnp.bfloat16
HIGH = lax.Precision.HIGHEST


def dot(a, b, dims=((1,), (0,)), precision=None):
    return lax.dot_general(
        a, b, (dims, ((), ())), precision=precision, preferred_element_type=F32
    )


def exact(a, b, dims=((1,), (0,))):
    return dot(a, b, dims, HIGH)


def vmem_call(body, outs, scratch=(), smem=0, cid=None, name=None):
    params = dict(vmem_limit_bytes=60 * 1024 * 1024)
    if cid is not None:
        params.update(collective_id=cid, has_side_effects=True)

    def call(*args):
        specs = [
            pl.BlockSpec(memory_space=pltpu.SMEM if k < smem else VMEM) for k in range(len(args))
        ]
        return pl.pallas_call(
            body,
            out_shape=tuple(jax.ShapeDtypeStruct(s, d) for s, d in outs),
            in_specs=specs,
            out_specs=tuple(pl.BlockSpec(memory_space=VMEM) for _ in outs),
            scratch_shapes=list(scratch),
            compiler_params=pltpu.CompilerParams(**params),
            name=name,
        )(*args)

    return call


def places(nz, ny):
    z, y, t = lax.axis_index("z"), lax.axis_index("y"), lax.axis_index("tp")

    def at(dz, dy):
        return (lax.rem(z + (dz + nz), nz), lax.rem(y + (dy + ny), ny), t)

    return z, y, at


def remote(src, dst, ssem, rsem, device):
    return pltpu.make_async_remote_copy(
        src_ref=src, dst_ref=dst, send_sem=ssem, recv_sem=rsem, device_id=device, device_id_type=MESH
    )


def meet(peers):
    barrier = pltpu.get_barrier_semaphore()
    for peer in peers:
        pl.semaphore_signal(barrier, inc=1, device_id=peer, device_id_type=MESH)
    pl.semaphore_wait(barrier, len(peers))


class Link:
    def __init__(self, sems, own):
        self.sems, self.own, self.sent = sems, own, []

    def start(self, step, src, dst, device):
        copy = remote(src, dst, self.sems.at[0, step], self.sems.at[1, step], device)
        copy.start()
        self.sent.append(copy)

    def arrived(self, step, dst):
        remote(dst, dst, self.sems.at[0, step], self.sems.at[1, step], self.own).wait_recv()

    def drain(self):
        for copy in self.sent:
            copy.wait_send()


def weights_kernel(nz, ny, wa, wb, oa, ob, local, ya, za_up, za_dn, zb_up, zb_dn, y_up, y_dn, y_far):
    z, y, at = places(nz, ny)
    up, down, left, right = at(1, 0), at(-1, 0), at(0, -1), at(0, 1)
    meet([up, down, left, right, at(0, 2)])
    row = lambda d: lax.rem(z + (d + nz), nz)
    col = lambda d: lax.rem(y + (d + ny), ny)
    ups, dns = nz // 2, nz // 2 - 1
    links = [Link(s, up) for s in (ya, za_up, za_dn, zb_up, zb_dn, y_up, y_dn, y_far)]
    ya, za_up, za_dn, zb_up, zb_dn, y_up, y_dn, y_far = links
    keep_a = pltpu.make_async_copy(wa, oa.at[z, y], local.at[0])
    keep_b = pltpu.make_async_copy(wb, ob.at[z, y], local.at[1])
    keep_a.start()
    keep_b.start()
    for d in (1, 3, 2):
        ya.start(d - 1, wa, oa.at[z, y], at(0, d))
    zb_up.start(0, wb, ob.at[z, y], up)
    zb_dn.start(0, wb, ob.at[z, y], down)

    def fan(k, zz, src):
        y_up.start(k, src, ob.at[zz, y], right)
        y_dn.start(k, src, ob.at[zz, y], left)

    def far(k, zz):
        y_up.arrived(k, ob.at[zz, col(-1)])
        y_dn.arrived(k, ob.at[zz, col(1)])
        if k % 2 == 0:
            y_far.start(k, ob.at[zz, col(-1)], ob.at[zz, col(-1)], right)
        else:
            y_far.start(k, ob.at[zz, col(1)], ob.at[zz, col(1)], left)

    fan(0, z, wb)
    for d in (1, 3, 2):
        ya.arrived(d - 1, oa.at[z, col(-d)])
    keep_a.wait()
    za_up.start(0, oa.at[z], oa.at[z], up)
    za_dn.start(0, oa.at[z], oa.at[z], down)
    waiting = [(0, z)]
    for s in range(ups):
        fresh = []
        for sign, steps, zb, za, to in ((-1, ups, zb_up, za_up, up), (1, dns, zb_dn, za_dn, down)):
            if s >= steps:
                continue
            zz = row(sign * (s + 1))
            zb.arrived(s, ob.at[zz, y])
            if s + 1 < steps:
                zb.start(s + 1, ob.at[zz, y], ob.at[zz, y], to)
            k = 2 * s + (1 if sign < 0 else 2)
            fan(k, zz, ob.at[zz, y])
            fresh.append((k, zz))
            za.arrived(s, oa.at[zz])
            if s + 1 < steps:
                za.start(s + 1, oa.at[zz], oa.at[zz], to)
        for k, zz in waiting:
            far(k, zz)
        waiting = fresh
    for k, zz in waiting:
        far(k, zz)
    for k in range(nz):
        y_far.arrived(k, ob.at[row(0), col(2)])
    keep_b.wait()
    for link in links:
        link.drain()


def gather_weights(nz, ny, wa, wb):
    sems = lambda n: pltpu.SemaphoreType.DMA((2, n))
    ups, dns = nz // 2, nz // 2 - 1
    return vmem_call(
        functools.partial(weights_kernel, nz, ny),
        [((nz, ny) + wa.shape, wa.dtype), ((nz, ny) + wb.shape, wb.dtype)],
        [pltpu.SemaphoreType.DMA((2,)), sems(ny - 1)]
        + [sems(ups), sems(dns)] * 2
        + [sems(nz)] * 3,
        cid=1,
        name="gather_weights",
    )(wa, wb)


def exchange_kernel(nz, ny, n_ring, n_all, n_swap, *refs):
    n = n_ring + n_all + n_swap
    ins, outs, sems = refs[:n], refs[n : 2 * n], refs[2 * n :]
    local, sems = sems[0], sems[1:]
    z, y, at = places(nz, ny)
    up, down = at(1, 0), at(-1, 0)
    row = lambda d: lax.rem(z + (d + nz), nz)
    col = lambda d: lax.rem(y + (d + ny), ny)
    ups, dns = nz // 2, nz // 2 - 1
    peers = [up, down] if n_ring else []
    if n_all + n_swap:
        peers += [at(0, d) for d in range(1, ny)]
    meet(peers)
    links, keeps, rings, flats = [], [], [], []
    for k in range(n):
        src, dst = ins[k], outs[k]
        if k < n_ring:
            up_link, dn_link = Link(sems[0], up), Link(sems[1], up)
            sems = sems[2:]
            up_link.start(0, src, dst.at[z], up)
            dn_link.start(0, src, dst.at[z], down)
            rings.append((dst, up_link, dn_link))
            links += [up_link, dn_link]
            keep = pltpu.make_async_copy(src, dst.at[z], local.at[k])
        else:
            link, sems = Link(sems[0], up), sems[1:]
            swap = k >= n_ring + n_all
            for d in (1, 3, 2):
                link.start(d - 1, src.at[col(d)] if swap else src, dst.at[y], at(0, d))
            flats.append((dst, link))
            links.append(link)
            keep = pltpu.make_async_copy(src.at[y] if swap else src, dst.at[y], local.at[k])
        keep.start()
        keeps.append(keep)
    if n_ring:
        for s in range(ups):
            for dst, up_link, dn_link in rings:
                for sign, steps, link, to in ((-1, ups, up_link, up), (1, dns, dn_link, down)):
                    if s >= steps:
                        continue
                    zz = row(sign * (s + 1))
                    link.arrived(s, dst.at[zz])
                    if s + 1 < steps:
                        link.start(s + 1, dst.at[zz], dst.at[zz], to)
    for dst, link in flats:
        for d in (1, 3, 2):
            link.arrived(d - 1, dst.at[col(-d)])
    for keep in keeps:
        keep.wait()
    for link in links:
        link.drain()


def exchange(nz, ny, cid, name, ring=(), all_y=(), swap_y=()):
    sems = lambda n: pltpu.SemaphoreType.DMA((2, n))
    outs = [((nz,) + a.shape, a.dtype) for a in ring]
    outs += [((ny,) + a.shape, a.dtype) for a in all_y]
    outs += [(a.shape, a.dtype) for a in swap_y]
    scratch = [pltpu.SemaphoreType.DMA((len(outs),))]
    for _ in ring:
        scratch += [sems(nz // 2), sems(nz // 2 - 1)]
    scratch += [sems(ny - 1)] * (len(all_y) + len(swap_y))
    return vmem_call(
        functools.partial(exchange_kernel, nz, ny, len(ring), len(all_y), len(swap_y)),
        outs,
        scratch,
        cid=cid,
        name=name,
    )(*ring, *all_y, *swap_y)


def iotas(shape):
    return lax.broadcasted_iota(jnp.int32, shape, 0), lax.broadcasted_iota(jnp.int32, shape, 1)


def softplus(x):
    return jnp.maximum(x, 0.0) + jnp.log1p(jnp.exp(-jnp.abs(x)))


def sigmoid(x):
    return 1.0 / (1.0 + jnp.exp(-x))


def unit_rows(values):
    return values * lax.rsqrt(jnp.sum(jnp.square(values), axis=-1, keepdims=True) + 1e-06)


def project_kernel(
    place, tok, gain, oa, ob, wbd, vec, extra, qt, kv, mb, solved_ref, qk_ref, qd_ref
):
    t = place[2]
    values = tok[...].astype(F32)
    center = jnp.mean(values, axis=-1, keepdims=True)
    shifted = values - center
    spread = jnp.mean(jnp.square(shifted), axis=-1, keepdims=True)
    normed = (shifted * lax.rsqrt(spread + 1e-05) * gain[...]).astype(BF16)
    attn = dot(normed, oa[...]).astype(BF16)
    delta = dot(normed, ob[:, : 3 * 128]).astype(BF16).astype(F32)
    gates = dot(normed, wbd[...]).astype(BF16).astype(F32)
    qt[...] = jnp.transpose(attn[:, :128].astype(F32)).astype(BF16)
    r, c = iotas((ROWS, ROWS))
    shuffle = jnp.where(c == (r & 7) * (ROWS // 8) + (r >> 3), 1.0, 0.0).astype(BF16)
    kv[0] = dot(shuffle, attn[:, 128:256]).astype(BF16)
    kv[1] = dot(shuffle, attn[:, 256:384]).astype(BF16)

    n_gate = wbd.shape[1] // 2
    lane = lax.broadcasted_iota(jnp.int32, (1, 2 * n_gate), 1)

    def pick(a, where):
        return jnp.sum(jnp.where(lane == where, a, 0.0), axis=-1, keepdims=True)

    beta = sigmoid(pick(gates, t) + pick(vec[...], t))
    rate = jnp.exp(pick(vec[...], n_gate + t))
    decay = -rate * softplus(pick(gates, n_gate + t)) + extra[...]
    silu = delta * sigmoid(delta)
    queries = unit_rows(silu[:, :128]) * (128.0**-0.5)
    keys = unit_rows(silu[:, 128:256])
    vals = silu[:, 256:]
    lower = r >= c
    total = exact(jnp.where(lower, 1.0, 0.0), jnp.broadcast_to(decay, (ROWS, 128)))
    across = jnp.transpose(total)[:1, :]
    total = total[:, :1]
    end = total[ROWS - 1 :, :]
    mask = jnp.where(lower, jnp.exp(jnp.where(lower, total - across, 0.0)), 0.0)
    keys_beta = keys * beta
    grown = jnp.exp(total)
    nmat = jnp.where(r > c, exact(keys_beta, keys, ((1,), (1,))) * mask, 0.0)
    near = jnp.where((r >> 3) == (c >> 3), nmat, 0.0)
    two = exact(near, near)
    four = exact(two, two)
    inv = jnp.where(r == c, 1.0, 0.0) - near
    inv = inv + exact(inv, two)
    inv = inv + exact(inv, four)
    for bit in range(3, 8):
        cross = ((r >> (bit + 1)) == (c >> (bit + 1))) & ((r >> bit) != (c >> bit))
        part = jnp.where(cross, nmat, 0.0)
        inv = inv - exact(inv, exact(part, inv))
    solved = exact(inv, jnp.concatenate([keys_beta * grown, vals * beta], axis=1))
    solved_ref[...] = solved
    qk_ref[...] = exact(queries, keys, ((1,), (1,))) * mask
    qd_ref[...] = queries * grown
    to_end = keys * jnp.exp(end - total)
    written = exact(to_end, solved, ((0,), (0,)))
    rr, cc = iotas((128, 256))
    mb[...] = jnp.where(cc < 128, jnp.where(rr == cc, jnp.exp(end), 0.0) - written, written)


def attend_kernel(place, bias, kv, qt, mbs, o_ref, l_ref, total_ref, before_ref):
    z, y = place[0], place[1]
    nz, ny = kv.shape[0], qt.shape[0]
    groups = ROWS // 8
    sub = lax.broadcasted_iota(jnp.int32, (8, ROWS), 0)
    query = lax.broadcasted_iota(jnp.int32, (8, ROWS), 1)

    def tile(zp, yq, masked):
        sums = []
        for h in range(2):
            scores = dot(kv[zp, 0, :, h * 64 : h * 64 + 64], qt[yq, h * 64 : h * 64 + 64, :])
            run = jnp.zeros((8, ROWS), F32)
            left = [None] * groups
            for g in reversed(range(groups)):
                u = scores[g * 8 : g * 8 + 8] * (0.125 * LOG2E) + bias[0, h] * LOG2E
                lost = jnp.maximum(u, jnp.log2(1.0 + jnp.exp2(jnp.minimum(u, 100.0))))
                if masked:
                    lost = jnp.where(sub * groups + g < query + ROWS * (yq - y), lost, 0.0)
                run = run + lost
                left[g] = u - run
            incl = run
            for d in (1, 2, 4):
                incl = incl + jnp.where(sub < 8 - d, pltpu.roll(incl, 8 - d, 0), 0.0)
            later = jnp.where(sub < 7, pltpu.roll(incl, 7, 0), 0.0)
            weights = []
            for g in range(groups):
                w = jnp.exp2(left[g] - later)
                if masked:
                    w = jnp.where(sub * groups + g < query + ROWS * (yq - y), w, 0.0)
                weights.append(w)
            weights = jnp.concatenate(weights, axis=0).astype(BF16)
            o_ref[zp, yq, h * 64 : h * 64 + 64, :] = dot(
                kv[zp, 1, :, h * 64 : h * 64 + 64], weights, ((0,), (0,))
            )
            sums.append(incl[:1])
        l_ref[zp, yq] = jnp.concatenate(sums, axis=0)

    l_ref[...] = jnp.zeros_like(l_ref)

    @pl.loop(0, z * ny)
    def _(k):
        tile(lax.div(k, ny), lax.rem(k, ny), False)

    @pl.loop(0, ny)
    def _(yq):
        tile(z, yq, True)

    rr, cc = iotas((128, 256))
    chain = jnp.where(rr == cc, 1.0, 0.0)
    before = chain
    for k in range(ny):
        m = mbs[k]
        before = jnp.where(y == k, chain, before)
        chain = exact(m[:, :128], chain) + jnp.where(cc < 128, 0.0, m)
    before_ref[...] = before
    total_ref[...] = chain


def combine_kernel(
    place, o_ref, l_ref, totals, before, solved, qk, qd, gain, part_ref, delta_ref, state
):
    z, y = place[0], place[1]
    ny = l_ref.shape[0]
    part_ref[...] = jnp.zeros_like(part_ref)

    def one(i, later):
        zp = z - i
        sums = [l_ref[k, zp] for k in range(ny)]
        here = later
        for k in range(ny):
            here = here + jnp.where(k > y, sums[k], 0.0)
            later = later + sums[k]
        kept = jnp.exp2(-here)
        for yq in range(ny):
            for h in range(2):
                rows = slice(h * 64, h * 64 + 64)
                part_ref[yq, rows, :] += o_ref[zp, yq, rows, :] * kept[yq, h : h + 1, :]
        return later

    lax.fori_loop(0, z + 1, one, jnp.zeros(l_ref.shape[2:], F32))
    state[...] = jnp.zeros_like(state)

    @pl.loop(0, z)
    def _(k):
        state[...] = exact(totals[k, :, :128], state[...]) + totals[k, :, 128:]

    incoming = exact(before[:, :128], state[...]) + before[:, 128:]
    fresh = solved[:, 128:] - exact(solved[:, :128], incoming)
    raw = exact(qd[...], incoming) + exact(qk[...], fresh)
    scale = lax.rsqrt(jnp.mean(jnp.square(raw), axis=-1, keepdims=True) + 1e-06)
    delta_ref[...] = (raw * scale * gain[...]).astype(BF16)


def output_kernel(parts, delta, gain, wo, out):
    raw = parts[0]
    for k in range(1, parts.shape[0]):
        raw = raw + parts[k]
    halves = []
    for h in range(2):
        half = raw[h * 64 : h * 64 + 64]
        halves.append(half * lax.rsqrt(jnp.mean(jnp.square(half), axis=0, keepdims=True) + 1e-06))
    attn = (jnp.transpose(jnp.concatenate(halves, axis=0)) * gain[...]).astype(BF16)
    mixed = jnp.concatenate([attn, delta[...]], axis=1)
    out[...] = dot(mixed, wo[...], ((1,), (1,))).astype(BF16)


def local(
    nz,
    ny,
    tokens,
    ln_gain,
    w_query_attn,
    w_key_attn,
    w_value_attn,
    w_query_delta,
    w_key_delta,
    w_value_delta,
    w_beta,
    w_decay,
    attn_bias,
    decay_log,
    beta_bias,
    log_decay_extra,
    attn_gain,
    delta_gain,
    w_out_attn,
    w_out_delta,
):
    z, y, t = lax.axis_index("z"), lax.axis_index("y"), lax.axis_index("tp")
    place = jnp.stack([z, y, t]).astype(jnp.int32)
    wa = jnp.concatenate([w_query_attn, w_key_attn, w_value_attn], axis=1)
    wb = jnp.concatenate(
        [w_query_delta, w_key_delta, w_value_delta, w_out_attn.T, w_out_delta.T], axis=1
    )
    oa, ob = gather_weights(nz, ny, wa, wb)
    oa = oa.reshape(-1, oa.shape[-1])
    ob = ob.reshape(-1, ob.shape[-1])
    wbd = jnp.concatenate([w_beta, w_decay], axis=1)
    vec = jnp.concatenate([beta_bias, decay_log])[None]
    qt, kv, mb, solved, qk, qd = vmem_call(
        project_kernel,
        [
            ((128, ROWS), BF16),
            ((2, ROWS, 128), BF16),
            ((128, 256), F32),
            ((ROWS, 256), F32),
            ((ROWS, ROWS), F32),
            ((ROWS, 128), F32),
        ],
        smem=1,
        name="project",
    )(place, tokens, ln_gain[None], oa, ob, wbd, vec, log_decay_extra)
    kvs, qts, mbs = exchange(nz, ny, 2, "gather_keys", ring=(kv,), all_y=(qt, mb))
    bias = lax.dynamic_slice_in_dim(attn_bias, 2 * t, 2, 0)[None]
    o, sums, total, before = vmem_call(
        attend_kernel,
        [
            ((nz, ny, 128, ROWS), F32),
            ((nz, ny, 2, ROWS), F32),
            ((128, 256), F32),
            ((128, 256), F32),
        ],
        smem=2,
        name="attend",
    )(place, bias, kvs, qts, mbs)
    totals, all_sums = exchange(nz, ny, 3, "gather_states", ring=(total,), all_y=(sums,))
    parts, delta = vmem_call(
        combine_kernel,
        [((ny, 128, ROWS), F32), ((ROWS, 128), BF16)],
        [pltpu.VMEM((128, 128), F32)],
        smem=1,
        name="combine",
    )(place, o, all_sums, totals, before, solved, qk, qd, delta_gain[None])
    (parts,) = exchange(nz, ny, 4, "swap_parts", swap_y=(parts,))
    gain2 = jnp.concatenate([attn_gain, attn_gain])[None]
    (partial,) = vmem_call(output_kernel, [((ROWS, ob.shape[0]), BF16)], name="output")(
        parts, delta, gain2, ob[:, 3 * 128 :]
    )
    n_tp = lax.axis_size("tp")
    pieces = partial.reshape(n_tp, ROWS // n_tp, -1)
    pieces = lax.all_to_all(pieces, "tp", 0, 0, tiled=True)
    return jnp.sum(pieces.astype(F32), axis=0).astype(BF16)


def solution(mesh):
    nz, ny = 16, 4
    split = Mesh(mesh.devices.reshape(nz, ny, mesh.shape["tp"]), ("z", "y", "tp"))
    return jax.shard_map(
        functools.partial(local, nz, ny),
        mesh=split,
        in_specs=(
            P(SP, None),
            P(),
            P(SP, "tp"),
            P(SP, "tp"),
            P(SP, "tp"),
            P(SP, "tp"),
            P(SP, "tp"),
            P(SP, "tp"),
            P(),
            P(),
            P(),
            P(),
            P(),
            P(SP, "tp"),
            P(),
            P(),
            P("tp", SP),
            P("tp", SP),
        ),
        out_specs=P(SP + ("tp",), None),
        check_vma=False,
    )
```

time: 832 us -> 259 us (0.31)
  waiting for transfers between devices: 397 us -> 0 us
  Pallas kernels: 0 us -> 206 us
  other arithmetic: 184 us -> 5.58 us
  matrix products: 93.2 us -> 0 us
  local copies, waits for them, and re-layouts: 67.3 us -> 8.88 us
  blocking collectives: 71.5 us -> 38 us
  between operations: 14.3 us -> 0.06 us
    all_gather x4 -> x0, waiting for transfers between devices: 397 us -> none  [the longest x2 275 us: side_by_side(): result = lax.all_gather(both, axis, axis=dim, tiled=True)]
    pallas_call x0 -> x8, Pallas kernels: none -> 206 us  [call(): pl.pallas_call(body, out_shape=tuple((jax.ShapeDtypeStruct(s, d) for s, d...]
    another operation x50 -> x1, other arithmetic: 103 us -> 0.59 us  [local(): place = jnp.stack([z, y, t]).astype(jnp.int32)]
    dot_general x101 -> x0, matrix products: 92.8 us -> none  [the longest x16 48.4 us: stick_block(): jnp.einsum('rhd,khd->hrk', queries, key_block.reshape(key_count, heads, h...]
    convert_element_type x20 -> x0, other arithmetic: 67.6 us -> none  [the longest x16 67.1 us: stick_block(): jnp.where(visible[None], jnp.exp(jax.nn.log_sigmoid(scores) + between), 0.0)]
    all_gather x3 -> x0, blocking collectives: 42.6 us -> none  [carried_in(): pieces = jax.tree.map(lambda part: lax.all_gather(part, axis), running)]
    another operation x49 -> x0, local copies, waits for them, and re-layouts: 30.9 us -> none  [the longest x16 30.7 us: stick_block(): lax.cumsum(lost, axis=2, reverse=True) - lost + log_kept[:, :, None]]
    dynamic_slice x27 -> x0, local copies, waits for them, and re-layouts: 23.1 us -> none  [the longest x16 17.1 us: one_turn(): lax.dynamic_slice_in_dim(values, block_index * block, block, 0)]
  transfers between devices with their start and end apart: 4 -> 0, of which waited for: 4 -> 0; matrix products, arithmetic and copies ran while one was open for 9% -> 0% of each run, Pallas kernels for 0% -> 0%
where the time goes in v1:
time: 259 us; the launch traced here: 258 us
  Pallas kernels  206 us (80%)
  blocking collectives  38 us (15%)
  local copies, waits for them, and re-layouts  8.88 us (3%)
  other arithmetic  5.58 us (2%)
    pallas_call x8, Pallas kernels, call(): pl.pallas_call(body, out_shape=tuple((jax.ShapeDtypeStruct(s, d) for s, d...  206 us
    all_to_all x1, blocking collectives, local(): pieces = lax.all_to_all(pieces, 'tp', 0, 0, tiled=True)  38 us

profile of v1, /device:TPU:1, one launch (start us, length us, event | category | flops | bytes accessed | tf_op | source)
XLA Modules:
  0.0 258.2 jit_solution(17382116648263041945)
XLA Ops:
  0.0 0.0 copy-start
  0.0 0.0 copy-start.3
  0.0 0.0 copy-start.2
  0.0 1.4 maximum_bitcast_fusion.1.gain
  1.4 0.7 constant_dynamic-update-slice_fusion.4
  2.1 1.5 copy.23.extra
  3.6 0.8 pad_maximum_fusion
  4.4 1.0 copy.22.wbd
  5.4 0.7 constant_dynamic-update-slice_fusion.3
  6.1 0.7 constant_dynamic-update-slice_fusion.2
  6.8 0.7 constant_dynamic-update-slice_fusion.1
  7.5 0.7 constant_dynamic-update-slice_fusion.wb
  8.2 0.0 copy-start.1
  8.2 1.4 pad_maximum_fusion.1.wa
  9.5 0.0 copy-done.1
  9.5 53.0 %gather_weights.1 = (bf16[16,4,32,384]{3,2,1,0:T(8,128)(2,1)}, bf16[16,4,32,640]{3,2,1,0:T(8,128)(2,1)}) custom-call(bf16[32,384]{1,0:T(8,128)(2,1)} %pad_maximum_fusion.1.wa, bf16[32,640]{1,0:T(8,128)(2,1)} %copy-done.1), custom_call_target="tpu_custom_call" | custom-call | tf_op jit(solution)/shard_map/gather_weights/pallas_call | solution.py:40
  62.6 2.3 slice.4.wo
  64.9 0.0 copy-done
  64.9 0.6 dynamic-slice_bitcast_fusion.bias
  65.5 0.0 copy-done.3
  65.5 0.0 copy-done.2
  65.5 0.6 maximum_bitcast_fusion.vec
  66.1 0.6 pad_add_fusion.place
  66.7 14.1 %project.1 = (bf16[128,256]{1,0:T(8,128)(2,1)}, bf16[2,256,128]{2,1,0:T(8,128)(2,1)}, f32[128,256]{1,0:T(8,128)}, f32[256,256]{1,0:T(8,128)}, f32[256,256]{1,0:T(8,128)}, /*index=5*/f32[256,128]{1,0:T(8,128)}) custom-call(s32[3]{0:T(128)} %pad_add_fusion.place, bf16[256,2048]{1,0:T(8,128)(2,1)} %tok.1, f32[1,2048]{1,0:T(1,128)} %bitcast.22, ...), custom_call_target="tpu_custom_call" | custom-call | tf_op jit(solution)/shard_map/project/pallas_call | solution.py:40
  80.8 34.3 %gather_keys.1 = (bf16[16,2,256,128]{3,2,1,0:T(8,128)(2,1)}, bf16[4,128,256]{2,1,0:T(8,128)(2,1)}, f32[4,128,256]{2,1,0:T(8,128)}) custom-call(bf16[2,256,128]{2,1,0:T(8,128)(2,1)} %get-tuple-element.26.refs_0_, bf16[128,256]{1,0:T(8,128)(2,1)} %get-tuple-element.27.refs_1_, f32[128,256]{1,0:T(8,128)} %get-tuple-element.28.refs_2_), custom_call_target="tpu_custom_call" | custom-call | tf_op jit(solution)/shard_map/gather_keys/pallas_call | solution.py:40
  115.1 8.5 %attend.1 = (f32[16,4,128,256]{3,2,1,0:T(8,128)}, f32[16,4,2,256]{3,2,1,0:T(2,128)}, f32[128,256]{1,0:T(8,128)}, f32[128,256]{1,0:T(8,128)}) custom-call(s32[3]{0:T(128)} %pad_add_fusion.place, f32[1,2]{1,0:T(1,128)} %dynamic-slice_bitcast_fusion.bias, bf16[16,2,256,128]{3,2,1,0:T(8,128)(2,1)} %get-tuple-element.29.kv, ...), custom_call_target="tpu_custom_call" | custom-call | tf_op jit(solution)/shard_map/attend/pallas_call | solution.py:40
  123.5 75.9 %gather_states.1 = (f32[16,128,256]{2,1,0:T(8,128)}, f32[4,16,4,2,256]{4,3,2,1,0:T(2,128)}) custom-call(f32[128,256]{1,0:T(8,128)} %get-tuple-element.33.refs_0_, f32[16,4,2,256]{3,2,1,0:T(2,128)} %get-tuple-element.34.refs_1_), custom_call_target="tpu_custom_call" | custom-call | tf_op jit(solution)/shard_map/gather_states/pallas_call | solution.py:40
  199.4 6.2 %combine.1 = (f32[4,128,256]{2,1,0:T(8,128)}, bf16[256,128]{1,0:T(8,128)(2,1)}) custom-call(s32[3]{0:T(128)} %pad_add_fusion.place, f32[16,4,128,256]{3,2,1,0:T(8,128)} %get-tuple-element.32.o_ref, f32[4,16,4,2,256]{4,3,2,1,0:T(2,128)} %get-tuple-element.35.l_ref, f32[16,128,256]{2,1,0:T(8,128)} %get-tuple-element.36.totals, ...), custom_call_target="tpu_custom_call" | custom-call | tf_op jit(solution)/shard_map/combine/pallas_call | solution.py:40
  205.6 10.9 %swap_parts.1.parts = f32[4,128,256]{2,1,0:T(8,128)} custom-call(f32[4,128,256]{2,1,0:T(8,128)} %get-tuple-element.41.refs_0_), custom_call_target="tpu_custom_call" | custom-call | tf_op jit(solution)/shard_map/swap_parts/pallas_call | solution.py:40
  216.5 2.9 %output.1 = bf16[256,2048]{1,0:T(8,128)(2,1)} custom-call(f32[4,128,256]{2,1,0:T(8,128)} %swap_parts.1.parts, bf16[256,128]{1,0:T(8,128)(2,1)} %get-tuple-element.42.delta, f32[1,128]{1,0:T(1,128)} %maximum_bitcast_fusion.1.gain, bf16[2048,256]{1,0:T(8,128)(2,1)} %slice.4.wo), custom_call_target="tpu_custom_call" | custom-call | tf_op jit(solution)/shard_map/output/pallas_call | solution.py:40
  219.4 38.0 %all_to_all.5 = bf16[8,32,2048]{2,1,0:T(8,128)(2,1)S(1)} all-to-all(bf16[8,32,2048]{2,1,0:T(8,128)(2,1)} %bitcast.20), channel_id=1, replica_groups=mesh['z'=16,'y'=4,'tp'=8] {'tp'}, dimensions={0} | all-to-all | bytes 2097152 | tf_op jit(solution)/shard_map/all_to_all | solution.py:497
  257.4 0.8 reduce_sum.12
Async XLA Ops:
  0.0 64.9 %copy-start = (f32[16]{0:T(128)S(1)}, f32[16]{0:T(128)}, u32[]{:S(2)}) copy-start(f32[16]{0:T(128)} %param.28) | copy-start | bytes 196
  0.0 65.5 %copy-start.3 = (f32[8]{0:T(128)S(1)}, f32[8]{0:T(128)}, u32[]{:S(2)}) copy-start(f32[8]{0:T(128)} %param.30) | copy-start | bytes 100
  0.0 65.5 %copy-start.2 = (f32[8]{0:T(128)S(1)}, f32[8]{0:T(128)}, u32[]{:S(2)}) copy-start(f32[8]{0:T(128)} %param.29) | copy-start | bytes 100
  8.2 1.4 copy-start.1

commit v2 on v1

v2 whole, which is shorter than its diff:
```python
import functools

import jax
import jax.numpy as jnp
from jax import lax
from jax.experimental import pallas as pl
from jax.experimental.pallas import tpu as pltpu
from jax.sharding import Mesh
from jax.sharding import PartitionSpec as P

MESH = pl.DeviceIdType.MESH
VMEM = pltpu.VMEM
SP = ("z", "y")
LOG2E = 1.4426950408889634
ROWS = 256
F32 = jnp.float32
BF16 = jnp.bfloat16
HIGH = lax.Precision.HIGHEST


def dot(a, b, dims=((1,), (0,)), precision=None):
    return lax.dot_general(
        a, b, (dims, ((), ())), precision=precision, preferred_element_type=F32
    )


def exact(a, b, dims=((1,), (0,))):
    return dot(a, b, dims, HIGH)


def split(a):
    high = a.astype(BF16)
    return high, (a - high.astype(F32)).astype(BF16)


def close(a, b, dims=((1,), (0,))):
    (ah, al), (bh, bl) = split(a), split(b)
    return dot(ah, bh, dims) + (dot(ah, bl, dims) + dot(al, bh, dims))


def apply_rounded(a, b):
    high, low = split(b)
    return dot(a, high) + dot(a, low)


def vmem_call(body, outs, scratch=(), smem=0, cid=None, name=None):
    params = dict(vmem_limit_bytes=60 * 1024 * 1024)
    if cid is not None:
        params.update(collective_id=cid, has_side_effects=True)

    def call(*args):
        specs = [
            pl.BlockSpec(memory_space=pltpu.SMEM if k < smem else VMEM) for k in range(len(args))
        ]
        return pl.pallas_call(
            body,
            out_shape=tuple(jax.ShapeDtypeStruct(s, d) for s, d in outs),
            in_specs=specs,
            out_specs=tuple(pl.BlockSpec(memory_space=VMEM) for _ in outs),
            scratch_shapes=list(scratch),
            compiler_params=pltpu.CompilerParams(**params),
            name=name,
        )(*args)

    return call


def places(nz, ny):
    z, y, t = lax.axis_index("z"), lax.axis_index("y"), lax.axis_index("tp")

    def at(dz, dy):
        return (lax.rem(z + (dz + nz), nz), lax.rem(y + (dy + ny), ny), t)

    return z, y, at


def remote(src, dst, ssem, rsem, device):
    return pltpu.make_async_remote_copy(
        src_ref=src, dst_ref=dst, send_sem=ssem, recv_sem=rsem, device_id=device, device_id_type=MESH
    )


def meet(peers):
    barrier = pltpu.get_barrier_semaphore()
    for peer in peers:
        pl.semaphore_signal(barrier, inc=1, device_id=peer, device_id_type=MESH)
    pl.semaphore_wait(barrier, len(peers))


class Link:
    def __init__(self, sems, own):
        self.sems, self.own, self.sent = sems, own, []

    def start(self, step, src, dst, device):
        copy = remote(src, dst, self.sems.at[0, step], self.sems.at[1, step], device)
        copy.start()
        self.sent.append(copy)

    def arrived(self, step, dst):
        remote(dst, dst, self.sems.at[0, step], self.sems.at[1, step], self.own).wait_recv()

    def drain(self):
        for copy in self.sent:
            copy.wait_send()


def weights_kernel(nz, ny, n_a, n_b, *refs):
    n = n_a + n_b
    ins, (oa, ob) = refs[:n], refs[n : n + 2]
    local, ya, za_up, za_dn, zb_up, zb_dn, y_up, y_dn, y_far = refs[n + 2 :]
    z, y, at = places(nz, ny)
    up, down, left, right = at(1, 0), at(-1, 0), at(0, -1), at(0, 1)
    row = lambda d: lax.rem(z + (d + nz), nz)
    col = lambda d: lax.rem(y + (d + ny), ny)
    ups, dns = nz // 2, nz // 2 - 1
    links = [Link(s, up) for s in (ya, za_up, za_dn, zb_up, zb_dn, y_up, y_dn, y_far)]
    ya, za_up, za_dn, zb_up, zb_dn, y_up, y_dn, y_far = links
    packs = []
    for k in range(n):
        out, place = (oa, k) if k < n_a else (ob, k - n_a)
        dst = out.at[z, y, :, pl.ds(128 * place, 128)]
        packs.append(pltpu.make_async_copy(ins[k], dst, local.at[k]))
        packs[-1].start()
    meet([up, down, left, right, at(0, 2)])
    for pack in packs:
        pack.wait()
    order = (0, 3, 1, 2)
    for d in (1, 3, 2):
        ya.start(d - 1, oa.at[z, y], oa.at[z, y], at(0, d))

    def lead(c):
        block = oa.at[z, col(c)]
        za_up.start(c, block, block, up)
        za_dn.start(c, block, block, down)

    def fan(k, zz):
        y_up.start(k, ob.at[zz, y], ob.at[zz, y], right)
        y_dn.start(k, ob.at[zz, y], ob.at[zz, y], left)

    def far(k, zz):
        y_up.arrived(k, ob.at[zz, col(-1)])
        y_dn.arrived(k, ob.at[zz, col(1)])
        if k % 2 == 0:
            y_far.start(k, ob.at[zz, col(-1)], ob.at[zz, col(-1)], right)
        else:
            y_far.start(k, ob.at[zz, col(1)], ob.at[zz, col(1)], left)

    lead(0)
    zb_up.start(0, ob.at[z, y], ob.at[z, y], up)
    zb_dn.start(0, ob.at[z, y], ob.at[z, y], down)
    fan(0, z)
    for c in order[1:]:
        ya.arrived(ny - c - 1, oa.at[z, col(c)])
        lead(c)
    waiting = [(0, z)]
    ways = ((-1, ups, zb_up, za_up, up), (1, dns, zb_dn, za_dn, down))
    for s in range(ups):
        fresh = []
        for c in order:
            for sign, steps, zb, za, to in ways:
                if s >= steps:
                    continue
                zz = row(sign * (s + 1))
                za.arrived(s * ny + c, oa.at[zz, col(c)])
                if s + 1 < steps:
                    za.start((s + 1) * ny + c, oa.at[zz, col(c)], oa.at[zz, col(c)], to)
                if c == 0:
                    zb.arrived(s, ob.at[zz, y])
                    if s + 1 < steps:
                        zb.start(s + 1, ob.at[zz, y], ob.at[zz, y], to)
                    k = 2 * s + (1 if sign < 0 else 2)
                    fan(k, zz)
                    fresh.append((k, zz))
        for k, zz in waiting:
            far(k, zz)
        waiting = fresh
    for k, zz in waiting:
        far(k, zz)
    for k in range(nz):
        y_far.arrived(k, ob.at[z, col(2)])
    for link in links:
        link.drain()


def gather_weights(nz, ny, set_a, set_b):
    sems = lambda n: pltpu.SemaphoreType.DMA((2, n))
    ups, dns = nz // 2, nz // 2 - 1
    n_a, n_b = len(set_a), len(set_b)
    rows, dtype = set_a[0].shape[0], set_a[0].dtype
    return vmem_call(
        functools.partial(weights_kernel, nz, ny, n_a, n_b),
        [((nz, ny, rows, 128 * n_a), dtype), ((nz, ny, rows, 128 * n_b), dtype)],
        [pltpu.SemaphoreType.DMA((n_a + n_b,)), sems(ny - 1), sems(ups * ny), sems(dns * ny)]
        + [sems(ups), sems(dns)]
        + [sems(nz)] * 3,
        cid=1,
        name="gather_weights",
    )(*set_a, *set_b)


def identity_part():
    rr, cc = iotas((128, 256))
    return jnp.where(rr == cc, 1.0, 0.0), cc < 128


def keys_kernel(nz, ny, *refs):
    kv, qt, mb, kvs, qts, mbs, totals, before = refs[:8]
    local, y_q, y_m, k_up, k_dn, t_up, t_dn = refs[8:]
    z, y, at = places(nz, ny)
    up, down = at(1, 0), at(-1, 0)
    row = lambda d: lax.rem(z + (d + nz), nz)
    col = lambda d: lax.rem(y + (d + ny), ny)
    ups, dns = nz // 2, nz // 2 - 1
    links = [Link(s, up) for s in (y_q, y_m, k_up, k_dn, t_up, t_dn)]
    y_q, y_m, k_up, k_dn, t_up, t_dn = links
    meet([up, down] + [at(0, d) for d in range(1, ny)])
    keeps = [
        pltpu.make_async_copy(kv, kvs.at[z], local.at[0]),
        pltpu.make_async_copy(qt, qts.at[y], local.at[1]),
        pltpu.make_async_copy(mb, mbs.at[y], local.at[2]),
    ]
    for d in (1, 3, 2):
        y_m.start(d - 1, mb, mbs.at[y], at(0, d))
    half = kv.shape[1] // 2
    part = lambda ref, p: ref.at[p // 2, pl.ds(half * (p % 2), half)]
    for p in range(4):
        k_up.start(p, part(kv, p), part(kvs.at[z], p), up)
        k_dn.start(p, part(kv, p), part(kvs.at[z], p), down)
    for d in (1, 3, 2):
        y_q.start(d - 1, qt, qts.at[y], at(0, d))
    for keep in keeps:
        keep.start()
    ways = ((-1, ups, k_up, t_up, up), (1, dns, k_dn, t_dn, down))
    t_rows = totals.shape[1] // 2
    piece = lambda zz, p: totals.at[zz, pl.ds(t_rows * p, t_rows)]
    lag = 2
    for s in range(ups + lag):
        for sign, steps, link, _, to in ways:
            if s < steps:
                zz = row(sign * (s + 1))
                for p in range(4):
                    block = part(kvs.at[zz], p)
                    link.arrived(4 * s + p, block)
                    if s + 1 < steps:
                        link.start(4 * (s + 1) + p, block, block, to)
        if s == 0:
            for d in (1, 3, 2):
                y_m.arrived(d - 1, mbs.at[col(-d)])
            keeps[2].wait()
            eye, left_half = identity_part()
            chain, first = eye, eye
            for k in range(ny):
                m = mbs[k]
                first = jnp.where(y == k, chain, first)
                shift = chain + jnp.where(left_half, 0.0, m.astype(F32))
                chain = apply_rounded(m[:, :128], chain) + shift
            before[...] = first
            totals[z] = (chain - eye).astype(BF16)
        if s == lag - 1:
            for p in range(2):
                t_up.start(p, piece(z, p), piece(z, p), up)
                t_dn.start(p, piece(z, p), piece(z, p), down)
        if s >= lag:
            for sign, steps, _, link, to in ways:
                if s - lag < steps:
                    zz = row(sign * (s - lag + 1))
                    for p in range(2):
                        link.arrived(2 * (s - lag) + p, piece(zz, p))
                        if s - lag + 1 < steps:
                            link.start(2 * (s - lag + 1) + p, piece(zz, p), piece(zz, p), to)
    for d in (1, 3, 2):
        y_q.arrived(d - 1, qts.at[col(-d)])
    keeps[0].wait()
    keeps[1].wait()
    for link in links:
        link.drain()


def gather_keys(nz, ny, kv, qt, mb):
    sems = lambda n: pltpu.SemaphoreType.DMA((2, n))
    ups, dns = nz // 2, nz // 2 - 1
    return vmem_call(
        functools.partial(keys_kernel, nz, ny),
        [
            ((nz,) + kv.shape, kv.dtype),
            ((ny,) + qt.shape, qt.dtype),
            ((ny,) + mb.shape, mb.dtype),
            ((nz,) + mb.shape, BF16),
            (mb.shape, F32),
        ],
        [pltpu.SemaphoreType.DMA((3,)), sems(ny - 1), sems(ny - 1)]
        + [sems(4 * ups), sems(4 * dns), sems(2 * ups), sems(2 * dns)],
        cid=2,
        name="gather_keys",
    )(kv, qt, mb)


def sums_kernel(ny, sums, every, local, y_s):
    _, y, at = places(1, ny)
    z = lax.axis_index("z")
    t = lax.axis_index("tp")
    col = lambda d: lax.rem(y + (d + ny), ny)
    peer = lambda d: (z, col(d), t)
    link = Link(y_s, peer(1))
    meet([peer(d) for d in range(1, ny)])
    for d in (1, 3, 2):
        link.start(d - 1, sums, every.at[y], peer(d))
    keep = pltpu.make_async_copy(sums, every.at[y], local.at[0])
    keep.start()
    for d in (1, 3, 2):
        link.arrived(d - 1, every.at[col(-d)])
    keep.wait()
    link.drain()


def gather_sums(ny, sums):
    return vmem_call(
        functools.partial(sums_kernel, ny),
        [((ny,) + sums.shape, sums.dtype)],
        [pltpu.SemaphoreType.DMA((1,)), pltpu.SemaphoreType.DMA((2, ny - 1))],
        cid=3,
        name="gather_sums",
    )(sums)[0]


def iotas(shape):
    return lax.broadcasted_iota(jnp.int32, shape, 0), lax.broadcasted_iota(jnp.int32, shape, 1)


def softplus(x):
    return jnp.maximum(x, 0.0) + jnp.log1p(jnp.exp(-jnp.abs(x)))


def sigmoid(x):
    return 1.0 / (1.0 + jnp.exp(-x))


def unit_rows(values):
    return values * lax.rsqrt(jnp.sum(jnp.square(values), axis=-1, keepdims=True) + 1e-06)


def project_kernel(
    place,
    tok,
    gain,
    oa,
    ob,
    w_beta,
    w_decay,
    beta_bias,
    decay_log,
    extra,
    qt,
    kv,
    mb,
    solved_ref,
    qk_ref,
    qd_ref,
):
    t = place[2]
    values = tok[...].astype(F32)
    center = jnp.mean(values, axis=-1, keepdims=True)
    shifted = values - center
    spread = jnp.mean(jnp.square(shifted), axis=-1, keepdims=True)
    normed = (shifted * lax.rsqrt(spread + 1e-05) * gain[...]).astype(BF16)
    attn = dot(normed, oa[...]).astype(BF16)
    delta = dot(normed, ob[:, : 3 * 128]).astype(BF16).astype(F32)
    beta_pre = dot(normed, w_beta[...], ((1,), (1,))).astype(BF16).astype(F32)
    decay_pre = dot(normed, w_decay[...], ((1,), (1,))).astype(BF16).astype(F32)
    qt[...] = jnp.transpose(attn[:, :128].astype(F32)).astype(BF16)
    r, c = iotas((ROWS, ROWS))
    shuffle = jnp.where(c == (r & 7) * (ROWS // 8) + (r >> 3), 1.0, 0.0).astype(BF16)
    kv[0] = dot(shuffle, attn[:, 128:256]).astype(BF16)
    kv[1] = dot(shuffle, attn[:, 256:384]).astype(BF16)

    lane = lax.broadcasted_iota(jnp.int32, (1, w_beta.shape[0]), 1)

    def pick(a):
        return jnp.sum(jnp.where(lane == t, a, 0.0), axis=-1, keepdims=True)

    beta = sigmoid(pick(beta_pre) + pick(beta_bias[...]))
    rate = jnp.exp(pick(decay_log[...]))
    added = jnp.transpose(jnp.broadcast_to(extra[...], (8, ROWS)))[:, :1]
    decay = -rate * softplus(pick(decay_pre)) + added
    silu = delta * sigmoid(delta)
    queries = unit_rows(silu[:, :128]) * (128.0**-0.5)
    keys = unit_rows(silu[:, 128:256])
    vals = silu[:, 256:]
    lower = r >= c
    total = exact(jnp.where(lower, 1.0, 0.0), jnp.broadcast_to(decay, (ROWS, 128)))
    across = jnp.transpose(total)[:1, :]
    total = total[:, :1]
    end = total[ROWS - 1 :, :]
    mask = jnp.where(lower, jnp.exp(jnp.where(lower, total - across, 0.0)), 0.0)
    keys_beta = keys * beta
    grown = jnp.exp(total)
    nmat = jnp.where(r > c, close(keys_beta, keys, ((1,), (1,))) * mask, 0.0)
    near = jnp.where((r >> 3) == (c >> 3), nmat, 0.0)
    two = close(near, near)
    four = close(two, two)
    inv = jnp.where(r == c, 1.0, 0.0) - near
    inv = inv + close(inv, two)
    inv = inv + close(inv, four)
    for bit in range(3, 8):
        cross = ((r >> (bit + 1)) == (c >> (bit + 1))) & ((r >> bit) != (c >> bit))
        part = jnp.where(cross, nmat, 0.0)
        inv = inv - close(inv, close(part, inv))
    solved = close(inv, jnp.concatenate([keys_beta * grown, vals * beta], axis=1))
    solved_ref[...] = solved
    qk_ref[...] = close(queries, keys, ((1,), (1,))) * mask
    qd_ref[...] = queries * grown
    to_end = keys * jnp.exp(end - total)
    written = close(to_end, solved, ((0,), (0,)))
    eye, left_half = identity_part()
    mb[...] = jnp.where(left_half, eye * (jnp.exp(end) - 1.0) - written, written).astype(BF16)


def attend_kernel(place, bias, kv, qt, o_ref, l_ref, s_even, s_odd, w_even, w_odd):
    z, y = place[0], place[1]
    ny = qt.shape[0]
    groups = ROWS // 8
    sub = lax.broadcasted_iota(jnp.int32, (8, ROWS), 0)
    query = lax.broadcasted_iota(jnp.int32, (8, ROWS), 1)

    def score(k, s):
        zp, yq = lax.div(k, ny), lax.rem(k, ny)
        for h in range(2):
            s[h] = dot(kv[zp, 0, :, h * 64 : h * 64 + 64], qt[yq, h * 64 : h * 64 + 64, :])

    def weigh(k, s, w, masked):
        zp, yq = lax.div(k, ny), lax.rem(k, ny)
        ahead = query + ROWS * (yq - y)
        sums = []
        for h in range(2):
            run = jnp.zeros((8, ROWS), F32)
            left = [None] * groups
            for g in reversed(range(groups)):
                u = s[h, g * 8 : g * 8 + 8, :] * (0.125 * LOG2E) + bias[0, h] * LOG2E
                lost = jnp.maximum(u, jnp.log2(1.0 + jnp.exp2(jnp.minimum(u, 100.0))))
                if masked:
                    lost = jnp.where(sub * groups + g < ahead, lost, 0.0)
                run = run + lost
                left[g] = u - run
            incl = run
            for d in (1, 2, 4):
                incl = incl + jnp.where(sub < 8 - d, pltpu.roll(incl, 8 - d, 0), 0.0)
            later = jnp.where(sub < 7, pltpu.roll(incl, 7, 0), 0.0)
            for g in range(0, groups, 2):
                pair = [jnp.exp2(left[j] - later) for j in (g, g + 1)]
                if masked:
                    pair = [
                        jnp.where(sub * groups + j < ahead, e, 0.0) for e, j in zip(pair, (g, g + 1))
                    ]
                w[h, g * 8 : g * 8 + 16, :] = jnp.concatenate(pair, axis=0).astype(BF16)
            sums.append(incl[:1])
        l_ref[zp, yq] = jnp.concatenate(sums, axis=0)

    def apply(k, w):
        zp, yq = lax.div(k, ny), lax.rem(k, ny)
        for h in range(2):
            o_ref[zp, yq, h * 64 : h * 64 + 64, :] = dot(
                kv[zp, 1, :, h * 64 : h * 64 + 64], w[h], ((0,), (0,))
            ).astype(o_ref.dtype)

    def sweep(first, last, masked):
        score(first, s_even)
        w_odd[...] = jnp.zeros_like(w_odd)

        @pl.loop(0, lax.div(last - first, 2))
        def _(m):
            k = first + 2 * m
            score(k + 1, s_odd)
            weigh(k, s_even, w_even, masked)
            apply(jnp.maximum(k - 1, first), w_odd)
            score(jnp.minimum(k + 2, last - 1), s_even)
            weigh(k + 1, s_odd, w_odd, masked)
            apply(k, w_even)

        apply(last - 1, w_odd)

    l_ref[...] = jnp.zeros_like(l_ref)

    @pl.when(z > 0)
    def _():
        sweep(0, z * ny, False)

    sweep(z * ny, z * ny + ny, True)


def combine_kernel(
    place, o_ref, l_ref, totals, before, solved, qk, qd, gain, part_ref, delta_ref, state, acc
):
    z, y = place[0], place[1]
    ny = l_ref.shape[0]
    acc[...] = jnp.zeros_like(acc)

    def one(i, later):
        zp = z - i
        sums = [l_ref[k, zp] for k in range(ny)]
        here = later
        for k in range(ny):
            here = here + jnp.where(k > y, sums[k], 0.0)
            later = later + sums[k]
        kept = jnp.exp2(-here)
        for yq in range(ny):
            for h in range(2):
                rows = slice(h * 64, h * 64 + 64)
                acc[yq, rows, :] += o_ref[zp, yq, rows, :].astype(F32) * kept[yq, h : h + 1, :]
        return later

    lax.fori_loop(0, z + 1, one, jnp.zeros(l_ref.shape[2:], F32))
    part_ref[...] = acc[...].astype(BF16)
    state[...] = jnp.zeros_like(state)

    @pl.loop(0, z)
    def _(k):
        now = state[...]
        state[...] = now + apply_rounded(totals[k, :, :128], now) + totals[k, :, 128:].astype(F32)

    incoming = close(before[:, :128], state[...]) + before[:, 128:]
    fresh = solved[:, 128:] - close(solved[:, :128], incoming)
    raw = close(qd[...], incoming) + close(qk[...], fresh)
    scale = lax.rsqrt(jnp.mean(jnp.square(raw), axis=-1, keepdims=True) + 1e-06)
    delta_ref[...] = (raw * scale * gain[...]).astype(BF16)


def finish_kernel(
    ny, n_x, parts, delta, gain, wo, out, got, mixed, mine, other, sum_ref, seen, local, y_p, c_p, x_p
):
    y, z, t = lax.axis_index("y"), lax.axis_index("z"), lax.axis_index("tp")
    x, c = lax.div(t, 2), lax.rem(t, 2)
    col = lambda d: lax.rem(y + (d + ny), ny)
    far = lambda d: lax.rem(x + (d + n_x), n_x)
    in_y = lambda d: (z, col(d), t)
    twin = (z, y, 2 * x + (1 - c))
    in_x = lambda d: (z, y, 2 * far(d) + c)
    y_p, c_p, x_p = Link(y_p, twin), Link(c_p, twin), Link(x_p, twin)
    meet([in_y(d) for d in range(1, ny)] + [twin] + [in_x(d) for d in range(1, n_x)])
    for d in (1, 3, 2):
        y_p.start(d - 1, parts.at[col(d)], got.at[y], in_y(d))
    rows = out.shape[0]
    mixed[:, :, :, 128:] = delta[...].reshape(n_x, 2, rows, 128)
    raw = parts[y].astype(F32)
    for d in (1, 3, 2):
        y_p.arrived(d - 1, got.at[col(-d)])
        raw = raw + got[col(-d)].astype(F32)
    halves = []
    for h in range(2):
        half = raw[h * 64 : h * 64 + 64]
        halves.append(half * lax.rsqrt(jnp.mean(jnp.square(half), axis=0, keepdims=True) + 1e-06))
    gains = jnp.concatenate([gain[...], gain[...]], axis=1)
    attn = (jnp.transpose(jnp.concatenate(halves, axis=0)) * gains).astype(BF16)
    mixed[:, :, :, :128] = attn.reshape(n_x, 2, rows, 128)

    def product(core):
        picked = mixed[:, core].reshape(n_x * rows, 256)
        return dot(picked, wo[:, 3 * 128 :], ((1,), (1,))).astype(BF16).reshape(n_x, rows, -1)

    mine[...] = product(1 - c)
    own = product(c)
    c_p.start(0, mine, other, twin)
    sum_ref[...] = own
    c_p.arrived(0, other)
    for d in (2, 1, 3):
        sum_ref[far(d)] = (sum_ref[far(d)].astype(F32) + other[far(d)].astype(F32)).astype(BF16)
    total = sum_ref[x].astype(F32) + other[x].astype(F32)
    for d in (2, 1, 3):
        x_p.start(d - 1, sum_ref.at[far(d)], seen.at[x], in_x(d))
    for d in (1, 3, 2):
        x_p.arrived(d - 1, seen.at[far(-d)])
        total = total + seen[far(-d)].astype(F32)
    out[...] = total.astype(BF16)
    for link in (y_p, c_p, x_p):
        link.drain()


def finish(ny, n_x, parts, delta, gain, wo):
    rows, wide = ROWS // (2 * n_x), wo.shape[0]
    sems = lambda n: pltpu.SemaphoreType.DMA((2, n))
    big = pltpu.VMEM((n_x, rows, wide), BF16)
    return vmem_call(
        functools.partial(finish_kernel, ny, n_x),
        [((rows, wide), BF16)],
        [
            pltpu.VMEM(parts.shape, parts.dtype),
            pltpu.VMEM((n_x, 2, rows, 256), BF16),
            big,
            big,
            big,
            big,
            pltpu.SemaphoreType.DMA((1,)),
            sems(ny - 1),
            sems(1),
            sems(n_x - 1),
        ],
        cid=4,
        name="finish",
    )(parts, delta, gain, wo)[0]


def local(
    nz,
    ny,
    tokens,
    ln_gain,
    w_query_attn,
    w_key_attn,
    w_value_attn,
    w_query_delta,
    w_key_delta,
    w_value_delta,
    w_beta,
    w_decay,
    attn_bias,
    decay_log,
    beta_bias,
    log_decay_extra,
    attn_gain,
    delta_gain,
    w_out_attn,
    w_out_delta,
):
    z, y, t = lax.axis_index("z"), lax.axis_index("y"), lax.axis_index("tp")
    place = jnp.stack([z, y, t]).astype(jnp.int32)
    oa, ob = gather_weights(
        nz,
        ny,
        (w_query_attn, w_key_attn, w_value_attn),
        (w_query_delta, w_key_delta, w_value_delta, w_out_attn.T, w_out_delta.T),
    )
    oa = oa.reshape(-1, oa.shape[-1])
    ob = ob.reshape(-1, ob.shape[-1])
    qt, kv, mb, solved, qk, qd = vmem_call(
        project_kernel,
        [
            ((128, ROWS), BF16),
            ((2, ROWS, 128), BF16),
            ((128, 256), BF16),
            ((ROWS, 256), F32),
            ((ROWS, ROWS), F32),
            ((ROWS, 128), F32),
        ],
        smem=1,
        name="project",
    )(
        place,
        tokens,
        ln_gain[None],
        oa,
        ob,
        w_beta.T,
        w_decay.T,
        beta_bias[None],
        decay_log[None],
        log_decay_extra.T,
    )
    kvs, qts, mbs, totals, before = gather_keys(nz, ny, kv, qt, mb)
    bias = lax.dynamic_slice_in_dim(attn_bias, 2 * t, 2, 0)[None]
    o, sums = vmem_call(
        attend_kernel,
        [((nz, ny, 128, ROWS), BF16), ((nz, ny, 2, ROWS), F32)],
        [pltpu.VMEM((2, ROWS, ROWS), F32)] * 2 + [pltpu.VMEM((2, ROWS, ROWS), BF16)] * 2,
        smem=2,
        name="attend",
    )(place, bias, kvs, qts)
    all_sums = gather_sums(ny, sums)
    parts, delta = vmem_call(
        combine_kernel,
        [((ny, 128, ROWS), BF16), ((ROWS, 128), BF16)],
        [pltpu.VMEM((128, 128), F32), pltpu.VMEM((ny, 128, ROWS), F32)],
        smem=1,
        name="combine",
    )(place, o, all_sums, totals, before, solved, qk, qd, delta_gain[None])
    return finish(ny, lax.axis_size("tp") // 2, parts, delta, attn_gain[None], ob)


def solution(mesh):
    nz, ny = 16, 4
    split = Mesh(mesh.devices.reshape(nz, ny, mesh.shape["tp"]), ("z", "y", "tp"))
    return jax.shard_map(
        functools.partial(local, nz, ny),
        mesh=split,
        in_specs=(
            P(SP, None),
            P(),
            P(SP, "tp"),
            P(SP, "tp"),
            P(SP, "tp"),
            P(SP, "tp"),
            P(SP, "tp"),
            P(SP, "tp"),
            P(),
            P(),
            P(),
            P(),
            P(),
            P(SP, "tp"),
            P(),
            P(),
            P("tp", SP),
            P("tp", SP),
        ),
        out_specs=P(SP + ("tp",), None),
        check_vma=False,
    )
```

time: 259 us -> 174 us (0.67)
  the two profiles are of different devices: /device:TPU:1 before, /device:TPU:481 now
where the time goes in v2:
time: 174 us; the launch traced here: 173 us
  Pallas kernels  171 us (98%)
  local copies, waits for them, and re-layouts  2.24 us (1%)
    pallas_call x7, Pallas kernels, call(): pl.pallas_call(body, out_shape=tuple((jax.ShapeDtypeStruct(s, d) for s, d...  171 us

profile of v2, /device:TPU:481, one launch (start us, length us, event | category | flops | bytes accessed | tf_op | source)
XLA Modules:
  0.0 173.5 jit_solution(16299295212233710390)
XLA Ops:
  0.0 0.0 copy-start
  0.0 0.6 pad_add_fusion.place
  0.6 0.1 copy-done
  0.7 0.6 dynamic-slice_bitcast_fusion.bias
  1.3 38.3 %gather_weights.1 = (bf16[16,4,32,384]{3,2,1,0:T(8,128)(2,1)}, bf16[16,4,32,640]{3,2,1,0:T(8,128)(2,1)}) custom-call(bf16[32,128]{1,0:T(8,128)(2,1)} %refs_0_.1, bf16[32,128]{1,0:T(8,128)(2,1)} %refs_1_.1, bf16[32,128]{1,0:T(8,128)(2,1)} %refs_2_.1, bf16[32,128]{1,0:T(8,128)(2,1)} %refs_3_.1, bf16[32,128]{1,0:T(8,128)(2,1)} %refs_4_.1, ...), custom_call_target="tpu_custom_call" | custom-call | tf_op jit(solution)/shard_map/gather_weights/pallas_call | solution.py:55
  39.6 11.3 %project.1 = (bf16[128,256]{1,0:T(8,128)(2,1)}, bf16[2,256,128]{2,1,0:T(8,128)(2,1)}, bf16[128,256]{1,0:T(8,128)(2,1)}, f32[256,256]{1,0:T(8,128)}, f32[256,256]{1,0:T(8,128)}, /*index=5*/f32[256,128]{1,0:T(8,128)}) custom-call(s32[3]{0:T(128)} %pad_add_fusion.place, bf16[256,2048]{1,0:T(8,128)(2,1)} %tok.1, f32[1,2048]{1,0:T(1,128)} %bitcast.22, ...), custom_call_target="tpu_custom_call" | custom-call | tf_op jit(solution)/shard_map/project/pallas_call | solution.py:55
  50.9 42.9 %gather_keys.1 = (bf16[16,2,256,128]{3,2,1,0:T(8,128)(2,1)}, bf16[4,128,256]{2,1,0:T(8,128)(2,1)}, bf16[4,128,256]{2,1,0:T(8,128)(2,1)}, bf16[16,128,256]{2,1,0:T(8,128)(2,1)}, f32[128,256]{1,0:T(8,128)}) custom-call(bf16[2,256,128]{2,1,0:T(8,128)(2,1)} %get-tuple-element.23.refs_0_, bf16[128,256]{1,0:T(8,128)(2,1)} %get-tuple-element.24.refs_1_, ...), custom_call_target="tpu_custom_call" | custom-call | tf_op jit(solution)/shard_map/gather_keys/pallas_call | solution.py:55
  93.8 27.7 %attend.1 = (bf16[16,4,128,256]{3,2,1,0:T(8,128)(2,1)}, f32[16,4,2,256]{3,2,1,0:T(2,128)}) custom-call(s32[3]{0:T(128)} %pad_add_fusion.place, f32[1,2]{1,0:T(1,128)} %dynamic-slice_bitcast_fusion.bias, bf16[16,2,256,128]{3,2,1,0:T(8,128)(2,1)} %get-tuple-element.26.kv, bf16[4,128,256]{2,1,0:T(8,128)(2,1)} %get-tuple-element.27.qt), custom_call_target="tpu_custom_call" | custom-call | tf_op jit(solution)/shard_map/attend/pallas_call | solution.py:55
  121.5 9.2 %gather_sums.1.l_ref = f32[4,16,4,2,256]{4,3,2,1,0:T(2,128)} custom-call(f32[16,4,2,256]{3,2,1,0:T(2,128)} %get-tuple-element.29.sums), custom_call_target="tpu_custom_call" | custom-call | tf_op jit(solution)/shard_map/gather_sums/pallas_call | solution.py:55
  130.7 8.1 %combine.1 = (bf16[4,128,256]{2,1,0:T(8,128)(2,1)}, bf16[256,128]{1,0:T(8,128)(2,1)}) custom-call(s32[3]{0:T(128)} %pad_add_fusion.place, bf16[16,4,128,256]{3,2,1,0:T(8,128)(2,1)} %get-tuple-element.28.o_ref, f32[4,16,4,2,256]{4,3,2,1,0:T(2,128)} %gather_sums.1.l_ref, bf16[16,128,256]{2,1,0:T(8,128)(2,1)} %get-tuple-element.30.totals, ...), custom_call_target="tpu_custom_call" | custom-call | tf_op jit(solution)/shard_map/combine/pallas_call | solution.py:55
  138.8 33.1 %finish.1 = bf16[32,2048]{1,0:T(8,128)(2,1)} custom-call(bf16[4,128,256]{2,1,0:T(8,128)(2,1)} %get-tuple-element.35.parts, bf16[256,128]{1,0:T(8,128)(2,1)} %get-tuple-element.36.delta, f32[1,64]{1,0:T(1,128)} %bitcast.29, bf16[2048,640]{1,0:T(8,128)(2,1)} %bitcast.18), custom_call_target="tpu_custom_call" | custom-call | tf_op jit(solution)/shard_map/finish/pallas_call | solution.py:55
  171.9 1.6 copy.20
Async XLA Ops:
  0.0 0.7 copy-start

commit v3 on v2

--- a/solution.py
+++ b/solution.py
@@ -203,126 +203,6 @@
     return jnp.where(rr == cc, 1.0, 0.0), cc < 128
 
 
-def keys_kernel(nz, ny, *refs):
-    kv, qt, mb, kvs, qts, mbs, totals, before = refs[:8]
-    local, y_q, y_m, k_up, k_dn, t_up, t_dn = refs[8:]
-    z, y, at = places(nz, ny)
-    up, down = at(1, 0), at(-1, 0)
-    row = lambda d: lax.rem(z + (d + nz), nz)
-    col = lambda d: lax.rem(y + (d + ny), ny)
-    ups, dns = nz // 2, nz // 2 - 1
-    links = [Link(s, up) for s in (y_q, y_m, k_up, k_dn, t_up, t_dn)]
-    y_q, y_m, k_up, k_dn, t_up, t_dn = links
-    meet([up, down] + [at(0, d) for d in range(1, ny)])
-    keeps = [
-        pltpu.make_async_copy(kv, kvs.at[z], local.at[0]),
-        pltpu.make_async_copy(qt, qts.at[y], local.at[1]),
-        pltpu.make_async_copy(mb, mbs.at[y], local.at[2]),
-    ]
-    for d in (1, 3, 2):
-        y_m.start(d - 1, mb, mbs.at[y], at(0, d))
-    half = kv.shape[1] // 2
-    part = lambda ref, p: ref.at[p // 2, pl.ds(half * (p % 2), half)]
-    for p in range(4):
-        k_up.start(p, part(kv, p), part(kvs.at[z], p), up)
-        k_dn.start(p, part(kv, p), part(kvs.at[z], p), down)
-    for d in (1, 3, 2):
-        y_q.start(d - 1, qt, qts.at[y], at(0, d))
-    for keep in keeps:
-        keep.start()
-    ways = ((-1, ups, k_up, t_up, up), (1, dns, k_dn, t_dn, down))
-    t_rows = totals.shape[1] // 2
-    piece = lambda zz, p: totals.at[zz, pl.ds(t_rows * p, t_rows)]
-    lag = 2
-    for s in range(ups + lag):
-        for sign, steps, link, _, to in ways:
-            if s < steps:
-                zz = row(sign * (s + 1))
-                for p in range(4):
-                    block = part(kvs.at[zz], p)
-                    link.arrived(4 * s + p, block)
-                    if s + 1 < steps:
-                        link.start(4 * (s + 1) + p, block, block, to)
-        if s == 0:
-            for d in (1, 3, 2):
-                y_m.arrived(d - 1, mbs.at[col(-d)])
-            keeps[2].wait()
-            eye, left_half = identity_part()
-            chain, first = eye, eye
-            for k in range(ny):
-                m = mbs[k]
-                first = jnp.where(y == k, chain, first)
-                shift = chain + jnp.where(left_half, 0.0, m.astype(F32))
-                chain = apply_rounded(m[:, :128], chain) + shift
-            before[...] = first
-            totals[z] = (chain - eye).astype(BF16)
-        if s == lag - 1:
-            for p in range(2):
-                t_up.start(p, piece(z, p), piece(z, p), up)
-                t_dn.start(p, piece(z, p), piece(z, p), down)
-        if s >= lag:
-            for sign, steps, _, link, to in ways:
-                if s - lag < steps:
-                    zz = row(sign * (s - lag + 1))
-                    for p in range(2):
-                        link.arrived(2 * (s - lag) + p, piece(zz, p))
-                        if s - lag + 1 < steps:
-                            link.start(2 * (s - lag + 1) + p, piece(zz, p), piece(zz, p), to)
-    for d in (1, 3, 2):
-        y_q.arrived(d - 1, qts.at[col(-d)])
-    keeps[0].wait()
-    keeps[1].wait()
-    for link in links:
-        link.drain()
-
-
-def gather_keys(nz, ny, kv, qt, mb):
-    sems = lambda n: pltpu.SemaphoreType.DMA((2, n))
-    ups, dns = nz // 2, nz // 2 - 1
-    return vmem_call(
-        functools.partial(keys_kernel, nz, ny),
-        [
-            ((nz,) + kv.shape, kv.dtype),
-            ((ny,) + qt.shape, qt.dtype),
-            ((ny,) + mb.shape, mb.dtype),
-            ((nz,) + mb.shape, BF16),
-            (mb.shape, F32),
-        ],
-        [pltpu.SemaphoreType.DMA((3,)), sems(ny - 1), sems(ny - 1)]
-        + [sems(4 * ups), sems(4 * dns), sems(2 * ups), sems(2 * dns)],
-        cid=2,
-        name="gather_keys",
-    )(kv, qt, mb)
-
-
-def sums_kernel(ny, sums, every, local, y_s):
-    _, y, at = places(1, ny)
-    z = lax.axis_index("z")
-    t = lax.axis_index("tp")
-    col = lambda d: lax.rem(y + (d + ny), ny)
-    peer = lambda d: (z, col(d), t)
-    link = Link(y_s, peer(1))
-    meet([peer(d) for d in range(1, ny)])
-    for d in (1, 3, 2):
-        link.start(d - 1, sums, every.at[y], peer(d))
-    keep = pltpu.make_async_copy(sums, every.at[y], local.at[0])
-    keep.start()
-    for d in (1, 3, 2):
-        link.arrived(d - 1, every.at[col(-d)])
-    keep.wait()
-    link.drain()
-
-
-def gather_sums(ny, sums):
-    return vmem_call(
-        functools.partial(sums_kernel, ny),
-        [((ny,) + sums.shape, sums.dtype)],
-        [pltpu.SemaphoreType.DMA((1,)), pltpu.SemaphoreType.DMA((2, ny - 1))],
-        cid=3,
-        name="gather_sums",
-    )(sums)[0]
-
-
 def iotas(shape):
     return lax.broadcasted_iota(jnp.int32, shape, 0), lax.broadcasted_iota(jnp.int32, shape, 1)
 
@@ -340,7 +220,6 @@
 
 
 def project_kernel(
-    place,
     tok,
     gain,
     oa,
@@ -357,7 +236,7 @@
     qk_ref,
     qd_ref,
 ):
-    t = place[2]
+    t = lax.axis_index("tp")
     values = tok[...].astype(F32)
     center = jnp.mean(values, axis=-1, keepdims=True)
     shifted = values - center
@@ -415,27 +294,108 @@
     mb[...] = jnp.where(left_half, eye * (jnp.exp(end) - 1.0) - written, written).astype(BF16)
 
 
-def attend_kernel(place, bias, kv, qt, o_ref, l_ref, s_even, s_odd, w_even, w_odd):
-    z, y = place[0], place[1]
-    ny = qt.shape[0]
+def mixer_kernel(
+    nz,
+    ny,
+    n_x,
+    bias,
+    kv,
+    qt,
+    mb,
+    solved,
+    qk,
+    qd,
+    delta_gain,
+    attn_gain,
+    wo,
+    seen,
+    kvs,
+    qts,
+    mbs,
+    totals,
+    before,
+    kept_o,
+    kept_l,
+    s_even,
+    s_odd,
+    w_even,
+    w_odd,
+    state,
+    acc,
+    parts,
+    got,
+    mixed,
+    mine,
+    other,
+    sum_ref,
+    local,
+    y_q,
+    y_m,
+    k_up,
+    k_dn,
+    t_up,
+    t_dn,
+    l_y,
+    y_p,
+    c_p,
+    x_p,
+):
+    z, y, at = places(nz, ny)
+    t = lax.axis_index("tp")
+    x, c = lax.div(t, 2), lax.rem(t, 2)
+    up, down = at(1, 0), at(-1, 0)
+    row = lambda d: lax.rem(z + (d + nz), nz)
+    col = lambda d: lax.rem(y + (d + ny), ny)
+    far = lambda d: lax.rem(x + (d + n_x), n_x)
+    in_y = lambda d: at(0, d)
+    twin = (z, y, 2 * x + (1 - c))
+    in_x = lambda d: (z, y, 2 * far(d) + c)
+    ups, dns = nz // 2, nz // 2 - 1
+    links = [Link(i, twin) for i in (y_q, y_m, t_up, t_dn, l_y, y_p, c_p, x_p)]
+    y_q, y_m, t_up, t_dn, l_y, y_p, c_p, x_p = links
+    k_up, k_dn = Link(k_up, twin), Link(k_dn, twin)
+    meet(
+        [up, down]
+        + [in_y(d) for d in range(1, ny)]
+        + [twin]
+        + [in_x(d) for d in range(1, n_x)]
+    )
+
+    half = kv.shape[1] // 2
+    part = lambda ref, p: ref.at[lax.div(p, 2), pl.ds(half * lax.rem(p, 2), half)]
+    for d in (1, 3, 2):
+        y_q.start(d - 1, qt, qts.at[y], in_y(d))
+    for p in range(4):
+        for link, to in ((k_up, up), (k_dn, down)):
+            piece = kv.at[p // 2, pl.ds(half * (p % 2), half)]
+            land = kvs.at[z, p // 2, pl.ds(half * (p % 2), half)]
+            link.start(p, piece, land, to)
+    keeps = [
+        pltpu.make_async_copy(kv, kvs.at[z], local.at[0]),
+        pltpu.make_async_copy(qt, qts.at[y], local.at[1]),
+        pltpu.make_async_copy(mb, mbs.at[y], local.at[2]),
+    ]
+    for keep in keeps:
+        keep.start()
+    for d in (1, 3, 2):
+        y_m.start(d - 1, mb, mbs.at[y], in_y(d))
+
     groups = ROWS // 8
     sub = lax.broadcasted_iota(jnp.int32, (8, ROWS), 0)
     query = lax.broadcasted_iota(jnp.int32, (8, ROWS), 1)
 
-    def score(k, s):
-        zp, yq = lax.div(k, ny), lax.rem(k, ny)
+    def score(zp, yq, s):
         for h in range(2):
-            s[h] = dot(kv[zp, 0, :, h * 64 : h * 64 + 64], qt[yq, h * 64 : h * 64 + 64, :])
-
-    def weigh(k, s, w, masked):
-        zp, yq = lax.div(k, ny), lax.rem(k, ny)
+            s[h] = dot(kvs[zp, 0, :, h * 64 : h * 64 + 64], qts[yq, h * 64 : h * 64 + 64, :])
+
+    def weigh(zp, yq, s, w, masked=False):
         ahead = query + ROWS * (yq - y)
         sums = []
         for h in range(2):
             run = jnp.zeros((8, ROWS), F32)
             left = [None] * groups
             for g in reversed(range(groups)):
-                u = s[h, g * 8 : g * 8 + 8, :] * (0.125 * LOG2E) + bias[0, h] * LOG2E
+                u = s[h, g * 8 : g * 8 + 8, :] * (0.125 * LOG2E) + bias[2 * t + h] * LOG2E
                 lost = jnp.maximum(u, jnp.log2(1.0 + jnp.exp2(jnp.minimum(u, 100.0))))
                 if masked:
                     lost = jnp.where(sub * groups + g < ahead, lost, 0.0)
@@ -453,50 +413,146 @@
                     ]
                 w[h, g * 8 : g * 8 + 16, :] = jnp.concatenate(pair, axis=0).astype(BF16)
             sums.append(incl[:1])
-        l_ref[zp, yq] = jnp.concatenate(sums, axis=0)
-
-    def apply(k, w):
-        zp, yq = lax.div(k, ny), lax.rem(k, ny)
+        kept_l[y, zp, yq] = jnp.concatenate(sums, axis=0)
+
+    def apply(zp, yq, w):
         for h in range(2):
-            o_ref[zp, yq, h * 64 : h * 64 + 64, :] = dot(
-                kv[zp, 1, :, h * 64 : h * 64 + 64], w[h], ((0,), (0,))
-            ).astype(o_ref.dtype)
-
-    def sweep(first, last, masked):
-        score(first, s_even)
-        w_odd[...] = jnp.zeros_like(w_odd)
-
-        @pl.loop(0, lax.div(last - first, 2))
-        def _(m):
-            k = first + 2 * m
-            score(k + 1, s_odd)
-            weigh(k, s_even, w_even, masked)
-            apply(jnp.maximum(k - 1, first), w_odd)
-            score(jnp.minimum(k + 2, last - 1), s_even)
-            weigh(k + 1, s_odd, w_odd, masked)
-            apply(k, w_even)
-
-        apply(last - 1, w_odd)
-
-    l_ref[...] = jnp.zeros_like(l_ref)
-
-    @pl.when(z > 0)
-    def _():
-        sweep(0, z * ny, False)
-
-    sweep(z * ny, z * ny + ny, True)
-
-
-def combine_kernel(
-    place, o_ref, l_ref, totals, before, solved, qk, qd, gain, part_ref, delta_ref, state, acc
-):
-    z, y = place[0], place[1]
-    ny = l_ref.shape[0]
+            kept_o[zp, yq, h * 64 : h * 64 + 64, :] = dot(
+                kvs[zp, 1, :, h * 64 : h * 64 + 64], w[h], ((0,), (0,))
+            )
+
+    def send_sums(block, zz):
+        for d in (1, 3, 2):
+            l_y.start(3 * block + d - 1, kept_l.at[y, zz], kept_l.at[y, zz], in_y(d))
+
+    def forward(s, p):
+        for sign, steps, link, to in ((-1, ups, k_up, up), (1, dns, k_dn, down)):
+            if s < steps:
+                block = part(kvs.at[row(sign * (s + 1))], p)
+                link.arrived(4 * s + p, block)
+                if s + 1 < steps:
+                    step = 4 * (s + 1) + p
+                    remote(block, block, link.sems.at[0, step], link.sems.at[1, step], to).start()
+
+    t_rows = totals.shape[1] // 2
+    piece = lambda zz, p: totals.at[zz, pl.ds(t_rows * p, t_rows)]
+
+    def forward_totals(j):
+        for sign, steps, link, to in ((-1, ups, t_up, up), (1, dns, t_dn, down)):
+            if j < steps:
+                zz = row(sign * (j + 1))
+                for p in range(2):
+                    link.arrived(2 * j + p, piece(zz, p))
+                    if j + 1 < steps:
+                        link.start(2 * (j + 1) + p, piece(zz, p), piece(zz, p), to)
+
+    @pl.loop(0, 4)
+    def _(p):
+        forward(0, p)
+
+    for d in (1, 3, 2):
+        y_q.arrived(d - 1, qts.at[col(-d)])
+    keeps[0].wait()
+    keeps[1].wait()
+    w_odd[...] = jnp.zeros_like(w_odd)
+    score(z, 0, s_even)
+
+    @pl.loop(0, ny // 2)
+    def _(m):
+        yq = 2 * m
+        score(z, yq + 1, s_odd)
+        weigh(z, yq, s_even, w_even, True)
+        apply(z, jnp.maximum(yq - 1, 0), w_odd)
+        score(z, jnp.minimum(yq + 2, ny - 1), s_even)
+        weigh(z, yq + 1, s_odd, w_odd, True)
+        apply(z, yq, w_even)
+
+    apply(z, ny - 1, w_odd)
+    score(row(-1), 0, s_even)
+
+    for s in range(1, ups):
+        if s == 1:
+            for d in (1, 3, 2):
+                y_m.arrived(d - 1, mbs.at[col(-d)])
+            keeps[2].wait()
+            eye, left_half = identity_part()
+            chain, first = eye, eye
+            for k in range(ny):
+                m = mbs[k]
+                first = jnp.where(y == k, chain, first)
+                shift = chain + jnp.where(left_half, 0.0, m.astype(F32))
+                chain = apply_rounded(m[:, :128], chain) + shift
+            before[...] = first
+            totals[z] = (chain - eye).astype(BF16)
+        one, two = row(-s), row(s)
+        last = two if s == 1 else row(s - 1)
+        ahead = row(-s - 1)
+
+        @pl.loop(0, ny)
+        def _(p):
+            forward(s, p)
+            at_start, at_end = p == 0, p == ny - 1
+            score(two, p, s_odd)
+            weigh(one, p, s_even, w_even)
+            apply(jnp.where(at_start, last, two), lax.rem(p + ny - 1, ny), w_odd)
+            score(jnp.where(at_end, ahead, one), lax.rem(p + 1, ny), s_even)
+            weigh(two, p, s_odd, w_odd)
+            apply(one, p, w_even)
+
+        if s == 1:
+            for p in range(2):
+                t_up.start(p, piece(z, p), piece(z, p), up)
+                t_dn.start(p, piece(z, p), piece(z, p), down)
+            send_sums(0, z)
+        else:
+            forward_totals(s - 2)
+            send_sums(2 * s - 3, row(1 - s))
+            send_sums(2 * s - 2, row(s - 1))
+
+    one, two = row(-ups), row(ups - 1)
+    score(one, 1, s_odd)
+    weigh(one, 0, s_even, w_even)
+    apply(two, ny - 1, w_odd)
+    send_sums(2 * ups - 3, row(1 - ups))
+    send_sums(2 * ups - 2, row(ups - 1))
+    forward_totals(ups - 2)
+    score(one, 2, s_even)
+    weigh(one, 1, s_odd, w_odd)
+    apply(one, 0, w_even)
+    score(one, 3, s_odd)
+    weigh(one, 2, s_even, w_even)
+    apply(one, 1, w_odd)
+    weigh(one, 3, s_odd, w_odd)
+    apply(one, 2, w_even)
+    apply(one, 3, w_odd)
+    forward_totals(ups - 1)
+    send_sums(2 * ups - 1, one)
+
+    state[...] = jnp.zeros_like(state)
+
+    @pl.loop(0, z)
+    def _(k):
+        now = state[...]
+        state[...] = now + apply_rounded(totals[k, :, :128], now) + totals[k, :, 128:].astype(F32)
+
+    incoming = close(before[:, :128], state[...]) + before[:, 128:]
+    fresh = solved[:, 128:] - close(solved[:, :128], incoming)
+    raw = close(qd[...], incoming) + close(qk[...], fresh)
+    scale = lax.rsqrt(jnp.mean(jnp.square(raw), axis=-1, keepdims=True) + 1e-06)
+    rows = seen.shape[1]
+    delta = (raw * scale * delta_gain[...]).astype(BF16)
+    mixed[:, :, :, 128:] = delta.reshape(n_x, 2, rows, 128)
+
+    blocks = [(0, z)] + [(1 + 2 * j, row(-1 - j)) for j in range(ups)]
+    blocks += [(2 + 2 * j, row(1 + j)) for j in range(dns)]
+    for block, zz in blocks:
+        for d in (1, 3, 2):
+            l_y.arrived(3 * block + d - 1, kept_l.at[col(-d), zz])
     acc[...] = jnp.zeros_like(acc)
 
-    def one(i, later):
+    def rescale(i, later):
         zp = z - i
-        sums = [l_ref[k, zp] for k in range(ny)]
+        sums = [kept_l[k, zp] for k in range(ny)]
         here = later
         for k in range(ny):
             here = here + jnp.where(k > y, sums[k], 0.0)
@@ -504,51 +560,24 @@
         kept = jnp.exp2(-here)
         for yq in range(ny):
             for h in range(2):
-                rows = slice(h * 64, h * 64 + 64)
-                acc[yq, rows, :] += o_ref[zp, yq, rows, :].astype(F32) * kept[yq, h : h + 1, :]
+                part_rows = slice(h * 64, h * 64 + 64)
+                acc[yq, part_rows, :] += kept_o[zp, yq, part_rows, :] * kept[yq, h : h + 1, :]
         return later
 
-    lax.fori_loop(0, z + 1, one, jnp.zeros(l_ref.shape[2:], F32))
-    part_ref[...] = acc[...].astype(BF16)
-    state[...] = jnp.zeros_like(state)
-
-    @pl.loop(0, z)
-    def _(k):
-        now = state[...]
-        state[...] = now + apply_rounded(totals[k, :, :128], now) + totals[k, :, 128:].astype(F32)
-
-    incoming = close(before[:, :128], state[...]) + before[:, 128:]
-    fresh = solved[:, 128:] - close(solved[:, :128], incoming)
-    raw = close(qd[...], incoming) + close(qk[...], fresh)
-    scale = lax.rsqrt(jnp.mean(jnp.square(raw), axis=-1, keepdims=True) + 1e-06)
-    delta_ref[...] = (raw * scale * gain[...]).astype(BF16)
-
-
-def finish_kernel(
-    ny, n_x, parts, delta, gain, wo, out, got, mixed, mine, other, sum_ref, seen, local, y_p, c_p, x_p
-):
-    y, z, t = lax.axis_index("y"), lax.axis_index("z"), lax.axis_index("tp")
-    x, c = lax.div(t, 2), lax.rem(t, 2)
-    col = lambda d: lax.rem(y + (d + ny), ny)
-    far = lambda d: lax.rem(x + (d + n_x), n_x)
-    in_y = lambda d: (z, col(d), t)
-    twin = (z, y, 2 * x + (1 - c))
-    in_x = lambda d: (z, y, 2 * far(d) + c)
-    y_p, c_p, x_p = Link(y_p, twin), Link(c_p, twin), Link(x_p, twin)
-    meet([in_y(d) for d in range(1, ny)] + [twin] + [in_x(d) for d in range(1, n_x)])
+    lax.fori_loop(0, z + 1, rescale, jnp.zeros(kept_l.shape[2:], F32))
+    parts[...] = acc[...].astype(BF16)
+    raw = acc[y]
     for d in (1, 3, 2):
         y_p.start(d - 1, parts.at[col(d)], got.at[y], in_y(d))
-    rows = out.shape[0]
-    mixed[:, :, :, 128:] = delta[...].reshape(n_x, 2, rows, 128)
-    raw = parts[y].astype(F32)
     for d in (1, 3, 2):
         y_p.arrived(d - 1, got.at[col(-d)])
         raw = raw + got[col(-d)].astype(F32)
     halves = []
     for h in range(2):
-        half = raw[h * 64 : h * 64 + 64]
-        halves.append(half * lax.rsqrt(jnp.mean(jnp.square(half), axis=0, keepdims=True) + 1e-06))
-    gains = jnp.concatenate([gain[...], gain[...]], axis=1)
+        piece_h = raw[h * 64 : h * 64 + 64]
+        power = jnp.mean(jnp.square(piece_h), axis=0, keepdims=True)
+        halves.append(piece_h * lax.rsqrt(power + 1e-06))
+    gains = jnp.concatenate([attn_gain[...], attn_gain[...]], axis=1)
     attn = (jnp.transpose(jnp.concatenate(halves, axis=0)) * gains).astype(BF16)
     mixed[:, :, :, :128] = attn.reshape(n_x, 2, rows, 128)
 
@@ -563,39 +592,65 @@
     c_p.arrived(0, other)
     for d in (2, 1, 3):
         sum_ref[far(d)] = (sum_ref[far(d)].astype(F32) + other[far(d)].astype(F32)).astype(BF16)
-    total = sum_ref[x].astype(F32) + other[x].astype(F32)
+    seen[x] = (sum_ref[x].astype(F32) + other[x].astype(F32)).astype(BF16)
     for d in (2, 1, 3):
         x_p.start(d - 1, sum_ref.at[far(d)], seen.at[x], in_x(d))
     for d in (1, 3, 2):
         x_p.arrived(d - 1, seen.at[far(-d)])
-        total = total + seen[far(-d)].astype(F32)
-    out[...] = total.astype(BF16)
-    for link in (y_p, c_p, x_p):
+    for link in links:
         link.drain()
-
-
-def finish(ny, n_x, parts, delta, gain, wo):
+    for link, steps in ((k_up, ups), (k_dn, dns)):
+
+        @pl.loop(0, 4 * steps)
+        def _(k):
+            block = part(kvs.at[z], lax.rem(k, 4))
+            remote(block, block, link.sems.at[0, k], link.sems.at[1, k], twin).wait_send()
+
+
+def mix(nz, ny, n_x, bias, kv, qt, mb, solved, qk, qd, delta_gain, attn_gain, wo):
     rows, wide = ROWS // (2 * n_x), wo.shape[0]
     sems = lambda n: pltpu.SemaphoreType.DMA((2, n))
     big = pltpu.VMEM((n_x, rows, wide), BF16)
+    ups, dns = nz // 2, nz // 2 - 1
     return vmem_call(
-        functools.partial(finish_kernel, ny, n_x),
-        [((rows, wide), BF16)],
+        functools.partial(mixer_kernel, nz, ny, n_x),
+        [((n_x, rows, wide), BF16)],
         [
-            pltpu.VMEM(parts.shape, parts.dtype),
+            pltpu.VMEM((nz,) + kv.shape, BF16),
+            pltpu.VMEM((ny,) + qt.shape, BF16),
+            pltpu.VMEM((ny,) + mb.shape, BF16),
+            pltpu.VMEM((nz,) + mb.shape, BF16),
+            pltpu.VMEM(mb.shape, F32),
+            pltpu.VMEM((nz, ny, 128, ROWS), F32),
+            pltpu.VMEM((ny, nz, ny, 2, ROWS), F32),
+            pltpu.VMEM((2, ROWS, ROWS), F32),
+            pltpu.VMEM((2, ROWS, ROWS), F32),
+            pltpu.VMEM((2, ROWS, ROWS), BF16),
+            pltpu.VMEM((2, ROWS, ROWS), BF16),
+            pltpu.VMEM((128, 128), F32),
+            pltpu.VMEM((ny, 128, ROWS), F32),
+            pltpu.VMEM((ny, 128, ROWS), BF16),
+            pltpu.VMEM((ny, 128, ROWS), BF16),
             pltpu.VMEM((n_x, 2, rows, 256), BF16),
             big,
             big,
             big,
-            big,
-            pltpu.SemaphoreType.DMA((1,)),
+            pltpu.SemaphoreType.DMA((3,)),
+            sems(ny - 1),
+            sems(ny - 1),
+            sems(4 * ups),
+            sems(4 * dns),
+            sems(2 * ups),
+            sems(2 * dns),
+            sems((ny - 1) * nz),
             sems(ny - 1),
             sems(1),
             sems(n_x - 1),
         ],
-        cid=4,
-        name="finish",
-    )(parts, delta, gain, wo)[0]
+        smem=1,
+        cid=2,
+        name="mixer",
+    )(bias, kv, qt, mb, solved, qk, qd, delta_gain, attn_gain, wo)[0]
 
 
 def local(
@@ -620,8 +675,6 @@
     w_out_attn,
     w_out_delta,
 ):
-    z, y, t = lax.axis_index("z"), lax.axis_index("y"), lax.axis_index("tp")
-    place = jnp.stack([z, y, t]).astype(jnp.int32)
     oa, ob = gather_weights(
         nz,
         ny,
@@ -640,10 +693,8 @@
             ((ROWS, ROWS), F32),
             ((ROWS, 128), F32),
         ],
-        smem=1,
         name="project",
     )(
-        place,
         tokens,
         ln_gain[None],
         oa,
@@ -654,24 +705,22 @@
         decay_log[None],
         log_decay_extra.T,
     )
-    kvs, qts, mbs, totals, before = gather_keys(nz, ny, kv, qt, mb)
-    bias = lax.dynamic_slice_in_dim(attn_bias, 2 * t, 2, 0)[None]
-    o, sums = vmem_call(
-        attend_kernel,
-        [((nz, ny, 128, ROWS), BF16), ((nz, ny, 2, ROWS), F32)],
-        [pltpu.VMEM((2, ROWS, ROWS), F32)] * 2 + [pltpu.VMEM((2, ROWS, ROWS), BF16)] * 2,
-        smem=2,
-        name="attend",
-    )(place, bias, kvs, qts)
-    all_sums = gather_sums(ny, sums)
-    parts, delta = vmem_call(
-        combine_kernel,
-        [((ny, 128, ROWS), BF16), ((ROWS, 128), BF16)],
-        [pltpu.VMEM((128, 128), F32), pltpu.VMEM((ny, 128, ROWS), F32)],
-        smem=1,
-        name="combine",
-    )(place, o, all_sums, totals, before, solved, qk, qd, delta_gain[None])
-    return finish(ny, lax.axis_size("tp") // 2, parts, delta, attn_gain[None], ob)
+    pieces = mix(
+        nz,
+        ny,
+        lax.axis_size("tp") // 2,
+        attn_bias,
+        kv,
+        qt,
+        mb,
+        solved,
+        qk,
+        qd,
+        delta_gain[None],
+        attn_gain[None],
+        ob,
+    )
+    return jnp.sum(pieces.astype(F32), axis=0).astype(BF16)
 
 
 def solution(mesh):

time: 174 us -> 139 us (0.80)
  the two profiles are of different devices: /device:TPU:481 before, /device:TPU:1 now
where the time goes in v3:
time: 139 us; the launch traced here: 138 us
  Pallas kernels  136 us (98%)
  other arithmetic  1.81 us (1%)
    pallas_call x3, Pallas kernels, call(): pl.pallas_call(body, out_shape=tuple((jax.ShapeDtypeStruct(s, d) for s, d...  136 us

profile of v3, /device:TPU:1, one launch (start us, length us, event | category | flops | bytes accessed | tf_op | source)
XLA Modules:
  0.0 138.3 jit_solution(3340596012097549655)
XLA Ops:
  0.0 47.9 %gather_weights.1 = (bf16[16,4,32,384]{3,2,1,0:T(8,128)(2,1)}, bf16[16,4,32,640]{3,2,1,0:T(8,128)(2,1)}) custom-call(bf16[32,128]{1,0:T(8,128)(2,1)} %refs_0_.1, bf16[32,128]{1,0:T(8,128)(2,1)} %refs_1_.1, bf16[32,128]{1,0:T(8,128)(2,1)} %refs_2_.1, bf16[32,128]{1,0:T(8,128)(2,1)} %refs_3_.1, bf16[32,128]{1,0:T(8,128)(2,1)} %refs_4_.1, ...), custom_call_target="tpu_custom_call" | custom-call | tf_op jit(solution)/shard_map/gather_weights/pallas_call | solution.py:55
  47.9 11.3 %project.1 = (bf16[128,256]{1,0:T(8,128)(2,1)}, bf16[2,256,128]{2,1,0:T(8,128)(2,1)}, bf16[128,256]{1,0:T(8,128)(2,1)}, f32[256,256]{1,0:T(8,128)}, f32[256,256]{1,0:T(8,128)}, /*index=5*/f32[256,128]{1,0:T(8,128)}) custom-call(bf16[256,2048]{1,0:T(8,128)(2,1)} %tok.1, f32[1,2048]{1,0:T(1,128)} %bitcast.17, bf16[2048,384]{1,0:T(8,128)(2,1)} %bitcast.14, ...), custom_call_target="tpu_custom_call" | custom-call | tf_op jit(solution)/shard_map/project/pallas_call | solution.py:55
  59.2 77.3 %mixer.1 = bf16[4,32,2048]{2,1,0:T(8,128)(2,1)} custom-call(f32[16]{0:T(128)} %bias.1, bf16[2,256,128]{2,1,0:T(8,128)(2,1)} %get-tuple-element.15.kv, bf16[128,256]{1,0:T(8,128)(2,1)} %get-tuple-element.16.qt, bf16[128,256]{1,0:T(8,128)(2,1)} %get-tuple-element.17.mb, f32[256,256]{1,0:T(8,128)} %get-tuple-element.18.solved, ...), custom_call_target="tpu_custom_call" | custom-call | tf_op jit(solution)/shard_map/mixer/pallas_call | solution.py:55
  136.5 1.8 %reduce_sum.12 = bf16[32,2048]{1,0:T(8,128)(2,1)} reduce(bf16[4,32,2048]{2,1,0:T(8,128)(2,1)} %mixer.1, bf16[]{:T(256)} %constant.2.clone.1), dimensions={0}, to_apply=%region_0.0 | reduce | flops 196608 | bytes 655362 | tf_op jit(solution)/shard_map/reduce_sum | solution.py:723

commit v4 on v3

--- a/solution.py
+++ b/solution.py
@@ -104,24 +104,112 @@
             copy.wait_send()
 
 
-def weights_kernel(nz, ny, n_a, n_b, *refs):
+def identity_part():
+    rr, cc = iotas((128, 256))
+    return jnp.where(rr == cc, 1.0, 0.0), cc < 128
+
+
+def iotas(shape):
+    return lax.broadcasted_iota(jnp.int32, shape, 0), lax.broadcasted_iota(jnp.int32, shape, 1)
+
+
+def softplus(x):
+    return jnp.maximum(x, 0.0) + jnp.log1p(jnp.exp(-jnp.abs(x)))
+
+
+def sigmoid(x):
+    return 1.0 / (1.0 + jnp.exp(-x))
+
+
+def unit_rows(values):
+    return values * lax.rsqrt(jnp.sum(jnp.square(values), axis=-1, keepdims=True) + 1e-06)
+
+
+SCRATCH = (
+    "oa",
+    "ob",
+    "normed",
+    "kvs",
+    "qts",
+    "mbs",
+    "totals",
+    "before",
+    "solved",
+    "qk_part",
+    "qd",
+    "kept_o",
+    "kept_l",
+    "s_even",
+    "s_odd",
+    "w_even",
+    "w_odd",
+    "state",
+    "acc",
+    "parts",
+    "got",
+    "mixed",
+    "mine",
+    "other",
+    "sum_ref",
+    "local",
+    "ya",
+    "za_up",
+    "za_dn",
+    "zb_up",
+    "zb_dn",
+    "y_up",
+    "y_dn",
+    "y_far",
+    "y_q",
+    "y_m",
+    "k_up",
+    "k_dn",
+    "t_up",
+    "t_dn",
+    "l_y",
+    "y_p",
+    "c_p",
+    "x_p",
+)
+
+
+def layer_kernel(nz, ny, n_x, n_a, n_b, attn_bias, tok, ln_gain, *refs):
     n = n_a + n_b
-    ins, (oa, ob) = refs[:n], refs[n : n + 2]
-    local, ya, za_up, za_dn, zb_up, zb_dn, y_up, y_dn, y_far = refs[n + 2 :]
+    ins, refs = refs[:n], refs[n:]
+    w_beta, w_decay, beta_bias, decay_log, extra, delta_gain, attn_gain, seen = refs[:8]
+    r_ = dict(zip(SCRATCH, refs[8:]))
+    oa, ob, normed_ref, kvs, qts, mbs, totals, before, solved, qk, qd = [
+        r_[k] for k in SCRATCH[:11]
+    ]
+    kept_o, kept_l, s_even, s_odd, w_even, w_odd = [r_[k] for k in SCRATCH[11:17]]
+    state, acc, parts, got, mixed, mine, other, sum_ref, local = [r_[k] for k in SCRATCH[17:26]]
     z, y, at = places(nz, ny)
+    t = lax.axis_index("tp")
+    x, c = lax.div(t, 2), lax.rem(t, 2)
     up, down, left, right = at(1, 0), at(-1, 0), at(0, -1), at(0, 1)
     row = lambda d: lax.rem(z + (d + nz), nz)
     col = lambda d: lax.rem(y + (d + ny), ny)
+    far = lambda d: lax.rem(x + (d + n_x), n_x)
+    in_y = lambda d: at(0, d)
+    twin = (z, y, 2 * x + (1 - c))
+    in_x = lambda d: (z, y, 2 * far(d) + c)
     ups, dns = nz // 2, nz // 2 - 1
-    links = [Link(s, up) for s in (ya, za_up, za_dn, zb_up, zb_dn, y_up, y_dn, y_far)]
-    ya, za_up, za_dn, zb_up, zb_dn, y_up, y_dn, y_far = links
+    every = {k: Link(r_[k], twin) for k in SCRATCH[26:]}
+    links = [every[k] for k in SCRATCH[26:] if k not in ("k_up", "k_dn")]
+    ya, za_up, za_dn, zb_up, zb_dn, y_up, y_dn, y_far = [every[k] for k in SCRATCH[26:34]]
+    y_q, y_m, k_up, k_dn, t_up, t_dn, l_y, y_p, c_p, x_p = [every[k] for k in SCRATCH[34:]]
     packs = []
     for k in range(n):
         out, place = (oa, k) if k < n_a else (ob, k - n_a)
         dst = out.at[z, y, :, pl.ds(128 * place, 128)]
         packs.append(pltpu.make_async_copy(ins[k], dst, local.at[k]))
         packs[-1].start()
-    meet([up, down, left, right, at(0, 2)])
+    meet(
+        [up, down]
+        + [in_y(d) for d in range(1, ny)]
+        + [twin]
+        + [in_x(d) for d in range(1, n_x)]
+    )
     for pack in packs:
         pack.wait()
     order = (0, 3, 1, 2)
@@ -137,7 +225,7 @@
         y_up.start(k, ob.at[zz, y], ob.at[zz, y], right)
         y_dn.start(k, ob.at[zz, y], ob.at[zz, y], left)
 
-    def far(k, zz):
+    def relay(k, zz):
         y_up.arrived(k, ob.at[zz, col(-1)])
         y_dn.arrived(k, ob.at[zz, col(1)])
         if k % 2 == 0:
@@ -149,22 +237,27 @@
     zb_up.start(0, ob.at[z, y], ob.at[z, y], up)
     zb_dn.start(0, ob.at[z, y], ob.at[z, y], down)
     fan(0, z)
-    for c in order[1:]:
-        ya.arrived(ny - c - 1, oa.at[z, col(c)])
-        lead(c)
+    values = tok[...].astype(F32)
+    center = jnp.mean(values, axis=-1, keepdims=True)
+    shifted = values - center
+    spread = jnp.mean(jnp.square(shifted), axis=-1, keepdims=True)
+    normed_ref[...] = (shifted * lax.rsqrt(spread + 1e-05) * ln_gain[...]).astype(BF16)
+    for c_ in order[1:]:
+        ya.arrived(ny - c_ - 1, oa.at[z, col(c_)])
+        lead(c_)
     waiting = [(0, z)]
     ways = ((-1, ups, zb_up, za_up, up), (1, dns, zb_dn, za_dn, down))
     for s in range(ups):
         fresh = []
-        for c in order:
+        for c_ in order:
             for sign, steps, zb, za, to in ways:
                 if s >= steps:
                     continue
                 zz = row(sign * (s + 1))
-                za.arrived(s * ny + c, oa.at[zz, col(c)])
+                za.arrived(s * ny + c_, oa.at[zz, col(c_)])
                 if s + 1 < steps:
-                    za.start((s + 1) * ny + c, oa.at[zz, col(c)], oa.at[zz, col(c)], to)
-                if c == 0:
+                    za.start((s + 1) * ny + c_, oa.at[zz, col(c_)], oa.at[zz, col(c_)], to)
+                if c_ == 0:
                     zb.arrived(s, ob.at[zz, y])
                     if s + 1 < steps:
                         zb.start(s + 1, ob.at[zz, y], ob.at[zz, y], to)
@@ -172,213 +265,32 @@
                     fan(k, zz)
                     fresh.append((k, zz))
         for k, zz in waiting:
-            far(k, zz)
+            relay(k, zz)
         waiting = fresh
     for k, zz in waiting:
-        far(k, zz)
+        relay(k, zz)
+
+    normed = normed_ref[...]
+    weights_a = oa[...].reshape(-1, 128 * n_a)
+    attn = dot(normed, weights_a).astype(BF16)
+    qts[y] = jnp.transpose(attn[:, :128].astype(F32)).astype(BF16)
+    r, c_ = iotas((ROWS, ROWS))
+    shuffle = jnp.where(c_ == (r & 7) * (ROWS // 8) + (r >> 3), 1.0, 0.0).astype(BF16)
+    kvs[z, 0] = dot(shuffle, attn[:, 128:256]).astype(BF16)
+    kvs[z, 1] = dot(shuffle, attn[:, 256:384]).astype(BF16)
+    beta_pre = dot(normed, w_beta[...], ((1,), (1,))).astype(BF16).astype(F32)
+    decay_pre = dot(normed, w_decay[...], ((1,), (1,))).astype(BF16).astype(F32)
     for k in range(nz):
         y_far.arrived(k, ob.at[z, col(2)])
-    for link in links:
-        link.drain()
-
-
-def gather_weights(nz, ny, set_a, set_b):
-    sems = lambda n: pltpu.SemaphoreType.DMA((2, n))
-    ups, dns = nz // 2, nz // 2 - 1
-    n_a, n_b = len(set_a), len(set_b)
-    rows, dtype = set_a[0].shape[0], set_a[0].dtype
-    return vmem_call(
-        functools.partial(weights_kernel, nz, ny, n_a, n_b),
-        [((nz, ny, rows, 128 * n_a), dtype), ((nz, ny, rows, 128 * n_b), dtype)],
-        [pltpu.SemaphoreType.DMA((n_a + n_b,)), sems(ny - 1), sems(ups * ny), sems(dns * ny)]
-        + [sems(ups), sems(dns)]
-        + [sems(nz)] * 3,
-        cid=1,
-        name="gather_weights",
-    )(*set_a, *set_b)
-
-
-def identity_part():
-    rr, cc = iotas((128, 256))
-    return jnp.where(rr == cc, 1.0, 0.0), cc < 128
-
-
-def iotas(shape):
-    return lax.broadcasted_iota(jnp.int32, shape, 0), lax.broadcasted_iota(jnp.int32, shape, 1)
-
-
-def softplus(x):
-    return jnp.maximum(x, 0.0) + jnp.log1p(jnp.exp(-jnp.abs(x)))
-
-
-def sigmoid(x):
-    return 1.0 / (1.0 + jnp.exp(-x))
-
-
-def unit_rows(values):
-    return values * lax.rsqrt(jnp.sum(jnp.square(values), axis=-1, keepdims=True) + 1e-06)
-
-
-def project_kernel(
-    tok,
-    gain,
-    oa,
-    ob,
-    w_beta,
-    w_decay,
-    beta_bias,
-    decay_log,
-    extra,
-    qt,
-    kv,
-    mb,
-    solved_ref,
-    qk_ref,
-    qd_ref,
-):
-    t = lax.axis_index("tp")
-    values = tok[...].astype(F32)
-    center = jnp.mean(values, axis=-1, keepdims=True)
-    shifted = values - center
-    spread = jnp.mean(jnp.square(shifted), axis=-1, keepdims=True)
-    normed = (shifted * lax.rsqrt(spread + 1e-05) * gain[...]).astype(BF16)
-    attn = dot(normed, oa[...]).astype(BF16)
-    delta = dot(normed, ob[:, : 3 * 128]).astype(BF16).astype(F32)
-    beta_pre = dot(normed, w_beta[...], ((1,), (1,))).astype(BF16).astype(F32)
-    decay_pre = dot(normed, w_decay[...], ((1,), (1,))).astype(BF16).astype(F32)
-    qt[...] = jnp.transpose(attn[:, :128].astype(F32)).astype(BF16)
-    r, c = iotas((ROWS, ROWS))
-    shuffle = jnp.where(c == (r & 7) * (ROWS // 8) + (r >> 3), 1.0, 0.0).astype(BF16)
-    kv[0] = dot(shuffle, attn[:, 128:256]).astype(BF16)
-    kv[1] = dot(shuffle, attn[:, 256:384]).astype(BF16)
-
-    lane = lax.broadcasted_iota(jnp.int32, (1, w_beta.shape[0]), 1)
-
-    def pick(a):
-        return jnp.sum(jnp.where(lane == t, a, 0.0), axis=-1, keepdims=True)
-
-    beta = sigmoid(pick(beta_pre) + pick(beta_bias[...]))
-    rate = jnp.exp(pick(decay_log[...]))
-    added = jnp.transpose(jnp.broadcast_to(extra[...], (8, ROWS)))[:, :1]
-    decay = -rate * softplus(pick(decay_pre)) + added
-    silu = delta * sigmoid(delta)
-    queries = unit_rows(silu[:, :128]) * (128.0**-0.5)
-    keys = unit_rows(silu[:, 128:256])
-    vals = silu[:, 256:]
-    lower = r >= c
-    total = exact(jnp.where(lower, 1.0, 0.0), jnp.broadcast_to(decay, (ROWS, 128)))
-    across = jnp.transpose(total)[:1, :]
-    total = total[:, :1]
-    end = total[ROWS - 1 :, :]
-    mask = jnp.where(lower, jnp.exp(jnp.where(lower, total - across, 0.0)), 0.0)
-    keys_beta = keys * beta
-    grown = jnp.exp(total)
-    nmat = jnp.where(r > c, close(keys_beta, keys, ((1,), (1,))) * mask, 0.0)
-    near = jnp.where((r >> 3) == (c >> 3), nmat, 0.0)
-    two = close(near, near)
-    four = close(two, two)
-    inv = jnp.where(r == c, 1.0, 0.0) - near
-    inv = inv + close(inv, two)
-    inv = inv + close(inv, four)
-    for bit in range(3, 8):
-        cross = ((r >> (bit + 1)) == (c >> (bit + 1))) & ((r >> bit) != (c >> bit))
-        part = jnp.where(cross, nmat, 0.0)
-        inv = inv - close(inv, close(part, inv))
-    solved = close(inv, jnp.concatenate([keys_beta * grown, vals * beta], axis=1))
-    solved_ref[...] = solved
-    qk_ref[...] = close(queries, keys, ((1,), (1,))) * mask
-    qd_ref[...] = queries * grown
-    to_end = keys * jnp.exp(end - total)
-    written = close(to_end, solved, ((0,), (0,)))
-    eye, left_half = identity_part()
-    mb[...] = jnp.where(left_half, eye * (jnp.exp(end) - 1.0) - written, written).astype(BF16)
-
-
-def mixer_kernel(
-    nz,
-    ny,
-    n_x,
-    bias,
-    kv,
-    qt,
-    mb,
-    solved,
-    qk,
-    qd,
-    delta_gain,
-    attn_gain,
-    wo,
-    seen,
-    kvs,
-    qts,
-    mbs,
-    totals,
-    before,
-    kept_o,
-    kept_l,
-    s_even,
-    s_odd,
-    w_even,
-    w_odd,
-    state,
-    acc,
-    parts,
-    got,
-    mixed,
-    mine,
-    other,
-    sum_ref,
-    local,
-    y_q,
-    y_m,
-    k_up,
-    k_dn,
-    t_up,
-    t_dn,
-    l_y,
-    y_p,
-    c_p,
-    x_p,
-):
-    z, y, at = places(nz, ny)
-    t = lax.axis_index("tp")
-    x, c = lax.div(t, 2), lax.rem(t, 2)
-    up, down = at(1, 0), at(-1, 0)
-    row = lambda d: lax.rem(z + (d + nz), nz)
-    col = lambda d: lax.rem(y + (d + ny), ny)
-    far = lambda d: lax.rem(x + (d + n_x), n_x)
-    in_y = lambda d: at(0, d)
-    twin = (z, y, 2 * x + (1 - c))
-    in_x = lambda d: (z, y, 2 * far(d) + c)
-    ups, dns = nz // 2, nz // 2 - 1
-    links = [Link(i, twin) for i in (y_q, y_m, t_up, t_dn, l_y, y_p, c_p, x_p)]
-    y_q, y_m, t_up, t_dn, l_y, y_p, c_p, x_p = links
-    k_up, k_dn = Link(k_up, twin), Link(k_dn, twin)
-    meet(
-        [up, down]
-        + [in_y(d) for d in range(1, ny)]
-        + [twin]
-        + [in_x(d) for d in range(1, n_x)]
-    )
-
-    half = kv.shape[1] // 2
+    half = ROWS // 2
     part = lambda ref, p: ref.at[lax.div(p, 2), pl.ds(half * lax.rem(p, 2), half)]
     for d in (1, 3, 2):
-        y_q.start(d - 1, qt, qts.at[y], in_y(d))
+        y_q.start(d - 1, qts.at[y], qts.at[y], in_y(d))
     for p in range(4):
         for link, to in ((k_up, up), (k_dn, down)):
-            piece = kv.at[p // 2, pl.ds(half * (p % 2), half)]
-            land = kvs.at[z, p // 2, pl.ds(half * (p % 2), half)]
-            link.start(p, piece, land, to)
-    keeps = [
-        pltpu.make_async_copy(kv, kvs.at[z], local.at[0]),
-        pltpu.make_async_copy(qt, qts.at[y], local.at[1]),
-        pltpu.make_async_copy(mb, mbs.at[y], local.at[2]),
-    ]
-    for keep in keeps:
-        keep.start()
-    for d in (1, 3, 2):
-        y_m.start(d - 1, mb, mbs.at[y], in_y(d))
+            block = kvs.at[z, p // 2, pl.ds(half * (p % 2), half)]
+            remote(block, block, link.sems.at[0, p], link.sems.at[1, p], to).start()
+    delta = dot(normed, ob[:, :, :, : 3 * 128].reshape(-1, 384)).astype(BF16).astype(F32)
 
     groups = ROWS // 8
     sub = lax.broadcasted_iota(jnp.int32, (8, ROWS), 0)
@@ -395,7 +307,7 @@
             run = jnp.zeros((8, ROWS), F32)
             left = [None] * groups
             for g in reversed(range(groups)):
-                u = s[h, g * 8 : g * 8 + 8, :] * (0.125 * LOG2E) + bias[2 * t + h] * LOG2E
+                u = s[h, g * 8 : g * 8 + 8, :] * (0.125 * LOG2E) + attn_bias[2 * t + h] * LOG2E
                 lost = jnp.maximum(u, jnp.log2(1.0 + jnp.exp2(jnp.minimum(u, 100.0))))
                 if masked:
                     lost = jnp.where(sub * groups + g < ahead, lost, 0.0)
@@ -446,14 +358,56 @@
                     if j + 1 < steps:
                         link.start(2 * (j + 1) + p, piece(zz, p), piece(zz, p), to)
 
+    lane = lax.broadcasted_iota(jnp.int32, (1, w_beta.shape[0]), 1)
+
+    def pick(a):
+        return jnp.sum(jnp.where(lane == t, a, 0.0), axis=-1, keepdims=True)
+
+    beta = sigmoid(pick(beta_pre) + pick(beta_bias[...]))
+    rate = jnp.exp(pick(decay_log[...]))
+    added = jnp.transpose(jnp.broadcast_to(extra[...], (8, ROWS)))[:, :1]
+    decay = -rate * softplus(pick(decay_pre)) + added
+    silu = delta * sigmoid(delta)
+    queries = unit_rows(silu[:, :128]) * (128.0**-0.5)
+    keys = unit_rows(silu[:, 128:256])
+    vals = silu[:, 256:]
+    lower = r >= c_
+    total = exact(jnp.where(lower, 1.0, 0.0), jnp.broadcast_to(decay, (ROWS, 128)))
+    across = jnp.transpose(total)[:1, :]
+    total = total[:, :1]
+    end = total[ROWS - 1 :, :]
+    mask = jnp.where(lower, jnp.exp(jnp.where(lower, total - across, 0.0)), 0.0)
+    keys_beta = keys * beta
+    grown = jnp.exp(total)
+    nmat = jnp.where(r > c_, close(keys_beta, keys, ((1,), (1,))) * mask, 0.0)
+    near = jnp.where((r >> 3) == (c_ >> 3), nmat, 0.0)
+    two = close(near, near)
+    four = close(two, two)
+    inv = jnp.where(r == c_, 1.0, 0.0) - near
+    inv = inv + close(inv, two)
+    inv = inv + close(inv, four)
+
     @pl.loop(0, 4)
     def _(p):
         forward(0, p)
 
+    for bit in range(3, 8):
+        cross = ((r >> (bit + 1)) == (c_ >> (bit + 1))) & ((r >> bit) != (c_ >> bit))
+        band = jnp.where(cross, nmat, 0.0)
+        inv = inv - close(inv, close(band, inv))
+    answer = close(inv, jnp.concatenate([keys_beta * grown, vals * beta], axis=1))
+    solved[...] = answer
+    to_end = keys * jnp.exp(end - total)
+    written = close(to_end, answer, ((0,), (0,)))
+    eye, left_half = identity_part()
+    mbs[y] = jnp.where(left_half, eye * (jnp.exp(end) - 1.0) - written, written).astype(BF16)
+    qk[...] = close(queries, keys, ((1,), (1,))) * mask
+    qd[...] = queries * grown
+    for d in (1, 3, 2):
+        y_m.start(d - 1, mbs.at[y], mbs.at[y], in_y(d))
+
     for d in (1, 3, 2):
         y_q.arrived(d - 1, qts.at[col(-d)])
-    keeps[0].wait()
-    keeps[1].wait()
     w_odd[...] = jnp.zeros_like(w_odd)
     score(z, 0, s_even)
 
@@ -474,7 +428,6 @@
         if s == 1:
             for d in (1, 3, 2):
                 y_m.arrived(d - 1, mbs.at[col(-d)])
-            keeps[2].wait()
             eye, left_half = identity_part()
             chain, first = eye, eye
             for k in range(ny):
@@ -583,7 +536,7 @@
 
     def product(core):
         picked = mixed[:, core].reshape(n_x * rows, 256)
-        return dot(picked, wo[:, 3 * 128 :], ((1,), (1,))).astype(BF16).reshape(n_x, rows, -1)
+        return dot(picked, ob[:, :, :, 3 * 128 :].reshape(-1, 256), ((1,), (1,))).astype(BF16).reshape(n_x, rows, -1)
 
     mine[...] = product(1 - c)
     own = product(c)
@@ -607,35 +560,52 @@
             remote(block, block, link.sems.at[0, k], link.sems.at[1, k], twin).wait_send()
 
 
-def mix(nz, ny, n_x, bias, kv, qt, mb, solved, qk, qd, delta_gain, attn_gain, wo):
-    rows, wide = ROWS // (2 * n_x), wo.shape[0]
+def layer(nz, ny, n_x, attn_bias, tok, ln_gain, set_a, set_b, *rest):
+    n_a, n_b = len(set_a), len(set_b)
+    w_rows, wide = set_a[0].shape[0], nz * ny * set_a[0].shape[0]
+    rows = ROWS // (2 * n_x)
     sems = lambda n: pltpu.SemaphoreType.DMA((2, n))
-    big = pltpu.VMEM((n_x, rows, wide), BF16)
+    f32 = lambda *shape: pltpu.VMEM(shape, F32)
+    b16 = lambda *shape: pltpu.VMEM(shape, BF16)
     ups, dns = nz // 2, nz // 2 - 1
     return vmem_call(
-        functools.partial(mixer_kernel, nz, ny, n_x),
+        functools.partial(layer_kernel, nz, ny, n_x, n_a, n_b),
         [((n_x, rows, wide), BF16)],
         [
-            pltpu.VMEM((nz,) + kv.shape, BF16),
-            pltpu.VMEM((ny,) + qt.shape, BF16),
-            pltpu.VMEM((ny,) + mb.shape, BF16),
-            pltpu.VMEM((nz,) + mb.shape, BF16),
-            pltpu.VMEM(mb.shape, F32),
-            pltpu.VMEM((nz, ny, 128, ROWS), F32),
-            pltpu.VMEM((ny, nz, ny, 2, ROWS), F32),
-            pltpu.VMEM((2, ROWS, ROWS), F32),
-            pltpu.VMEM((2, ROWS, ROWS), F32),
-            pltpu.VMEM((2, ROWS, ROWS), BF16),
-            pltpu.VMEM((2, ROWS, ROWS), BF16),
-            pltpu.VMEM((128, 128), F32),
-            pltpu.VMEM((ny, 128, ROWS), F32),
-            pltpu.VMEM((ny, 128, ROWS), BF16),
-            pltpu.VMEM((ny, 128, ROWS), BF16),
-            pltpu.VMEM((n_x, 2, rows, 256), BF16),
-            big,
-            big,
-            big,
-            pltpu.SemaphoreType.DMA((3,)),
+            b16(nz, ny, w_rows, 128 * n_a),
+            b16(nz, ny, w_rows, 128 * n_b),
+            b16(ROWS, wide),
+            b16(nz, 2, ROWS, 128),
+            b16(ny, 128, ROWS),
+            b16(ny, 128, 256),
+            b16(nz, 128, 256),
+            f32(128, 256),
+            f32(ROWS, 256),
+            f32(ROWS, ROWS),
+            f32(ROWS, 128),
+            f32(nz, ny, 128, ROWS),
+            f32(ny, nz, ny, 2, ROWS),
+            f32(2, ROWS, ROWS),
+            f32(2, ROWS, ROWS),
+            b16(2, ROWS, ROWS),
+            b16(2, ROWS, ROWS),
+            f32(128, 128),
+            f32(ny, 128, ROWS),
+            b16(ny, 128, ROWS),
+            b16(ny, 128, ROWS),
+            b16(n_x, 2, rows, 256),
+            b16(n_x, rows, wide),
+            b16(n_x, rows, wide),
+            b16(n_x, rows, wide),
+            pltpu.SemaphoreType.DMA((n_a + n_b,)),
+            sems(ny - 1),
+            sems(ups * ny),
+            sems(dns * ny),
+            sems(ups),
+            sems(dns),
+            sems(nz),
+            sems(nz),
+            sems(nz),
             sems(ny - 1),
             sems(ny - 1),
             sems(4 * ups),
@@ -648,9 +618,9 @@
             sems(n_x - 1),
         ],
         smem=1,
-        cid=2,
-        name="mixer",
-    )(bias, kv, qt, mb, solved, qk, qd, delta_gain, attn_gain, wo)[0]
+        cid=1,
+        name="layer",
+    )(attn_bias, tok, ln_gain, *set_a, *set_b, *rest)[0]
 
 
 def local(
@@ -675,50 +645,22 @@
     w_out_attn,
     w_out_delta,
 ):
-    oa, ob = gather_weights(
+    pieces = layer(
         nz,
         ny,
+        lax.axis_size("tp") // 2,
+        attn_bias,
+        tokens,
+        ln_gain[None],
         (w_query_attn, w_key_attn, w_value_attn),
         (w_query_delta, w_key_delta, w_value_delta, w_out_attn.T, w_out_delta.T),
-    )
-    oa = oa.reshape(-1, oa.shape[-1])
-    ob = ob.reshape(-1, ob.shape[-1])
-    qt, kv, mb, solved, qk, qd = vmem_call(
-        project_kernel,
-        [
-            ((128, ROWS), BF16),
-            ((2, ROWS, 128), BF16),
-            ((128, 256), BF16),
-            ((ROWS, 256), F32),
-            ((ROWS, ROWS), F32),
-            ((ROWS, 128), F32),
-        ],
-        name="project",
-    )(
-        tokens,
-        ln_gain[None],
-        oa,
-        ob,
         w_beta.T,
         w_decay.T,
         beta_bias[None],
         decay_log[None],
         log_decay_extra.T,
-    )
-    pieces = mix(
-        nz,
-        ny,
-        lax.axis_size("tp") // 2,
-        attn_bias,
-        kv,
-        qt,
-        mb,
-        solved,
-        qk,
-        qd,
         delta_gain[None],
         attn_gain[None],
-        ob,
     )
     return jnp.sum(pieces.astype(F32), axis=0).astype(BF16)
 

time: 139 us -> 125 us (0.90)
  Pallas kernels: 136 us -> 123 us
    pallas_call x3 -> x1, Pallas kernels: 136 us -> 123 us  [call(): pl.pallas_call(body, out_shape=tuple((jax.ShapeDtypeStruct(s, d) for s, d...]
where the time goes in v4:
time: 125 us
  Pallas kernels  123 us (98%)
  other arithmetic  1.81 us (1%)
    pallas_call x1, Pallas kernels, call(): pl.pallas_call(body, out_shape=tuple((jax.ShapeDtypeStruct(s, d) for s, d...  123 us

profile of v4, /device:TPU:1, one launch (start us, length us, event | category | flops | bytes accessed | tf_op | source)
XLA Modules:
  0.0 124.9 jit_solution(13133348116444980732)
XLA Ops:
  0.0 123.1 %layer.1 = bf16[4,32,2048]{2,1,0:T(8,128)(2,1)} custom-call(f32[16]{0:T(128)} %attn_bias.1, bf16[256,2048]{1,0:T(8,128)(2,1)} %tok.1, f32[1,2048]{1,0:T(1,128)} %bitcast.12, bf16[32,128]{1,0:T(8,128)(2,1)} %refs_0_.1, bf16[32,128]{1,0:T(8,128)(2,1)} %refs_1_.1, bf16[32,128]{1,0:T(8,128)(2,1)} %refs_2_.1, bf16[32,128]{1,0:T(8,128)(2,1)} %refs_3_.1, ...), custom_call_target="tpu_custom_call" | custom-call | tf_op jit(solution)/shard_map/layer/pallas_call | solution.py:55
  123.1 1.8 %reduce_sum.12 = bf16[32,2048]{1,0:T(8,128)(2,1)} reduce(bf16[4,32,2048]{2,1,0:T(8,128)(2,1)} %layer.1, bf16[]{:T(256)} %constant.2.clone.1), dimensions={0}, to_apply=%region_0.0 | reduce | flops 196608 | bytes 655362 | tf_op jit(solution)/shard_map/reduce_sum | solution.py:665

commit v5 on v4

--- a/solution.py
+++ b/solution.py
@@ -380,18 +380,28 @@
     keys_beta = keys * beta
     grown = jnp.exp(total)
     nmat = jnp.where(r > c_, close(keys_beta, keys, ((1,), (1,))) * mask, 0.0)
-    near = jnp.where((r >> 3) == (c_ >> 3), nmat, 0.0)
-    two = close(near, near)
-    four = close(two, two)
-    inv = jnp.where(r == c_, 1.0, 0.0) - near
-    inv = inv + close(inv, two)
-    inv = inv + close(inv, four)
+    r6, c6 = iotas((64, 64))
+    cuts = [slice(64 * b, 64 * b + 64) for b in range(ROWS // 64)]
+    own_n = [nmat[b, b] for b in cuts]
+    near = [jnp.where((r6 >> 3) == (c6 >> 3), m, 0.0) for m in own_n]
+    two = [close(m, m) for m in near]
+    four = [close(m, m) for m in two]
+    invs = [jnp.where(r6 == c6, 1.0, 0.0) - m for m in near]
+    invs = [a + close(a, m) for a, m in zip(invs, two)]
+    invs = [a + close(a, m) for a, m in zip(invs, four)]
+    for bit in range(3, 6):
+        cross = ((r6 >> (bit + 1)) == (c6 >> (bit + 1))) & ((r6 >> bit) != (c6 >> bit))
+        bands = [jnp.where(cross, m, 0.0) for m in own_n]
+        bands = [close(m, a) for m, a in zip(bands, invs)]
+        invs = [a - close(a, m) for a, m in zip(invs, bands)]
+    inv = jnp.concatenate([jnp.concatenate([a] * len(cuts), axis=1) for a in invs], axis=0)
+    inv = jnp.where((r >> 6) == (c_ >> 6), inv, 0.0)
 
     @pl.loop(0, 4)
     def _(p):
         forward(0, p)
 
-    for bit in range(3, 8):
+    for bit in range(6, 8):
         cross = ((r >> (bit + 1)) == (c_ >> (bit + 1))) & ((r >> bit) != (c_ >> bit))
         band = jnp.where(cross, nmat, 0.0)
         inv = inv - close(inv, close(band, inv))

time: 125 us -> 124 us (level)
  no operation moved by 1% of the time
where the time goes in v5:
time: 124 us
  Pallas kernels  122 us (98%)
  other arithmetic  1.81 us (1%)
    pallas_call x1, Pallas kernels, call(): pl.pallas_call(body, out_shape=tuple((jax.ShapeDtypeStruct(s, d) for s, d...  122 us

profile of v5, /device:TPU:1, one launch (start us, length us, event | category | flops | bytes accessed | tf_op | source)
XLA Modules:
  0.0 123.7 jit_solution(10234821418134732674)
XLA Ops:
  0.0 121.9 %layer.1 = bf16[4,32,2048]{2,1,0:T(8,128)(2,1)} custom-call(f32[16]{0:T(128)} %attn_bias.1, bf16[256,2048]{1,0:T(8,128)(2,1)} %tok.1, f32[1,2048]{1,0:T(1,128)} %bitcast.12, bf16[32,128]{1,0:T(8,128)(2,1)} %refs_0_.1, bf16[32,128]{1,0:T(8,128)(2,1)} %refs_1_.1, bf16[32,128]{1,0:T(8,128)(2,1)} %refs_2_.1, bf16[32,128]{1,0:T(8,128)(2,1)} %refs_3_.1, ...), custom_call_target="tpu_custom_call" | custom-call | tf_op jit(solution)/shard_map/layer/pallas_call | solution.py:55
  121.9 1.8 %reduce_sum.12 = bf16[32,2048]{1,0:T(8,128)(2,1)} reduce(bf16[4,32,2048]{2,1,0:T(8,128)(2,1)} %layer.1, bf16[]{:T(256)} %constant.2.clone.1), dimensions={0}, to_apply=%region_0.0 | reduce | flops 196608 | bytes 655362 | tf_op jit(solution)/shard_map/reduce_sum | solution.py:675
